TPU v7x, 256 devices: a whole 4x4x8 slice. The times are simulated.
256 devices in a mesh: sp: 32 (over z, y), fs: 4 (over x), tp: 2 (over core).
Axes of the slice: x: 4, y: 4, z: 8, core: 2. Of those that a mesh axis runs over, the one named last changes fastest.
Arguments:
- hidden_in: bfloat16 [4, 8192, 2048], P('fs', 'sp', 'tp'), may hold values from -6 to 6
- sb_query_w: bfloat16 [2048, 1024], P('fs', 'tp'), may hold values from -0.21875 to 0.21875
- sb_key_w: bfloat16 [2048, 1024], P('fs', 'tp'), may hold values from -0.21875 to 0.21875
- sb_value_w: bfloat16 [2048, 1024], P('fs', 'tp'), may hold values from -0.125 to 0.125
- sb_offset: float32 [16], P('tp'), may hold values from -16 to -6
- delta_query_w: bfloat16 [2048, 1024], P('fs', 'tp'), may hold values from -0.125 to 0.125
- delta_key_w: bfloat16 [2048, 1024], P('fs', 'tp'), may hold values from -0.125 to 0.125
- delta_value_w: bfloat16 [2048, 1024], P('fs', 'tp'), may hold values from -0.125 to 0.125
- decay_w: bfloat16 [2048, 8], P(None, 'tp'), may hold values from -0.125 to 0.125
- write_w: bfloat16 [2048, 8], P(None, 'tp'), may hold values from -0.125 to 0.125
- write_bias: float32 [8], P('tp'), may hold values from -7 to 1.5
- decay_log_scale: float32 [8], P('tp'), may hold values from -14 to -3
- decay_shift: float32 [4, 8, 8192], P('fs', 'tp', 'sp'), may hold values from -3 to 0
- head_gain: float32 [128], replicated, may hold values from 0.1 to 1.9
- sb_out_w: bfloat16 [1024, 2048], P('tp'), may hold values from -0.125 to 0.125
- delta_out_w: bfloat16 [1024, 2048], P('tp'), may hold values from -0.125 to 0.125
Outputs:
- mixed_out: bfloat16 [4, 8192, 2048], P('fs', ('sp', 'tp'))
All inputs are finite; a program needn't handle non-finite values.
Results may differ from a plain program's by a relative error of at most 0.015.
Values may be sent and summed in bfloat16 or wider, within the bound.
No kernel may reach another device: no remote copies, remote signals or barrier semaphores. Data moves between devices by JAX's collectives and lax.ppermute only.
A program may use at most 128 MiB of HBM per device.

v0:
```python
import functools

import jax
import jax.numpy as jnp
import numpy as np
from jax import lax
from jax.experimental import pallas as pl
from jax.experimental.pallas import tpu as pltpu
from jax.sharding import Mesh
from jax.sharding import PartitionSpec as P


f32 = jnp.float32
bf16 = jnp.bfloat16
LOG2E = float(np.log2(np.e))
EPS = 1e-6
CH = 256
NT = (((1,), (1,)), ((), ()))
Z = ("zh", "zl")
AXES = ("zh", "zl", "y", "fs", "tp")


SLOT = (0, 2, 4, 6, 7, 5, 3, 1)
PAIRS, SINGLE, SLOTS, COUNT, HEAD = 0, 256, 320, 328, 329


def work_list():
    table = np.zeros((32, 384), np.int32)
    for z in range(8):
        slot = lambda i: SLOT[(i - z) % 8]
        for y in range(4):
            row = table[4 * z + y]
            place = lambda i, m: (m % 4) * 8 + slot((4 * i + y - m) // 4)
            steps = [(slot(2 * p), slot(2 * p + 1), place(2 * p, m)) for p in (3, 2, 1, 0) for m in range(1, 8 * p + y + 1)]
            for n, step in enumerate(steps):
                for k in range(3):
                    row[PAIRS + 64 * k + n] = step[k]
            for chain, ps in enumerate(((3, 1), (2, 0))):
                steps_one = [(slot(2 * p + 1), place(2 * p + 1, m)) for p in ps for m in range(1, 5)]
                for n, step in enumerate(steps_one):
                    row[SINGLE + 16 * chain + n] = step[0]
                    row[SINGLE + 16 * chain + 8 + n] = step[1]
            row[SLOTS : SLOTS + 8] = [slot(i) for i in range(8)]
            row[COUNT], row[HEAD] = len(steps), z
    return table


def stick_kernel(table, off_ref, q, u_ref, *refs):
    kv_refs, o_ref, (acc, run, kvs, kt, late_a, late_b, sp_a, sp_b) = refs[:4], refs[4], refs[5:]
    off = off_ref[table[HEAD]] * LOG2E
    for d in range(4):
        for n in range(8):
            block = kv_refs[d][n]
            kvs[d * 8 + n] = block
            kt[d * 8 + n] = jnp.transpose(block)

    def tile(slots, c, masked):
        size = CH * len(slots)
        join = lambda ref: jnp.concatenate([ref[s] for s in slots], axis=0) if len(slots) > 1 else ref[slots[0]]
        kv = kvs[c]
        z = jnp.dot(join(q), kt[c], preferred_element_type=f32) * (0.125 * LOG2E) + off
        sp = jnp.maximum(jnp.log2(1.0 + jnp.exp2(jnp.minimum(z, 40.0))), z)
        if masked:
            shape = (size, CH)
            seen = lax.broadcasted_iota(jnp.int32, shape, 1) < lax.broadcasted_iota(jnp.int32, shape, 0)
            sp = jnp.where(seen, sp, 0.0)
        after = jnp.dot(sp.astype(bf16), u_ref[...], preferred_element_type=f32)
        total = after[:, :1] + sp[:, :1]
        if masked:
            w = jnp.where(seen, jnp.exp2((z - sp) - after), 0.0)
            total = jnp.broadcast_to(total, (size, 128))
            out = jnp.dot(w.astype(bf16), kv, preferred_element_type=f32)
        else:
            r = join(run)
            w = jnp.exp2((z - sp) - (after + jnp.concatenate([r, r], axis=1)))
            total = r + total
            out = join(acc) + jnp.dot(w.astype(bf16), kv, preferred_element_type=f32)
        for k, s in enumerate(slots):
            run[s] = total[k * CH : k * CH + CH]
            acc[s] = out[k * CH : k * CH + CH]

    def diagonal(n, carry):
        for k in range(2):
            tile((2 * n + k,), 2 * n + k, True)
        return carry

    lax.fori_loop(0, 4, diagonal, 0)

    def one(n, carry):
        for k in range(2):
            tile((table[SINGLE + 16 * k + n],), table[SINGLE + 16 * k + 8 + n], False)
        return carry

    lax.fori_loop(0, 8, one, 0)

    def step(n):
        return (table[PAIRS + n], table[PAIRS + 64 + n]), table[PAIRS + 128 + n]

    def scores(n, late, sp_at):
        slots, c = step(n)
        z = jnp.dot(jnp.concatenate([q[s] for s in slots]), kt[c], preferred_element_type=f32) * (0.125 * LOG2E) + off
        sp = jnp.maximum(jnp.log2(1.0 + jnp.exp2(jnp.minimum(z, 40.0))), z)
        late[...] = z - sp
        sp_at[...] = sp.astype(bf16)

    def weigh(n, late, sp_at):
        slots, c = step(n)
        after = jnp.dot(sp_at[...], u_ref[...], preferred_element_type=f32)
        r = jnp.concatenate([run[s] for s in slots])
        w = jnp.exp2(late[...] - (after + jnp.concatenate([r, r], axis=1)))
        out = jnp.dot(w.astype(bf16), kvs[c], preferred_element_type=f32)
        total = r + (after[:, :1] + sp_at[:, :1].astype(f32))
        for k, s in enumerate(slots):
            rows = slice(k * CH, k * CH + CH)
            run[s] = total[rows]
            acc[s] += out[rows]

    scores(0, late_a, sp_a)

    def two(m, carry):
        weigh(2 * m, late_a, sp_a)
        scores(2 * m + 1, late_b, sp_b)
        weigh(2 * m + 1, late_b, sp_b)
        scores(2 * m + 2, late_a, sp_a)
        return carry

    lax.fori_loop(0, table[COUNT] // 2, two, 0)
    lane = lax.broadcasted_iota(jnp.int32, (64, 128), 1)
    for i in range(8):
        rows = acc[table[SLOTS + i]]
        for h in range(2):
            low, high = rows[128 * h : 128 * h + 64], rows[128 * h + 64 : 128 * h + 128]
            o_ref[2 * i + h] = jnp.where(lane < 64, pltpu.roll(low, 64, 1), high).astype(bf16)


def stick_attention(table, off, q, u, kvs):
    smem = pl.BlockSpec(memory_space=pltpu.SMEM)
    vmem = pl.BlockSpec(memory_space=pltpu.VMEM)
    return pl.pallas_call(
        stick_kernel,
        out_shape=jax.ShapeDtypeStruct((16, 64, 128), bf16),
        in_specs=[smem] * 2 + [vmem] * 6,
        out_specs=vmem,
        scratch_shapes=[
            pltpu.VMEM((8, CH, 128), f32),
            pltpu.VMEM((8, CH, 128), f32),
            pltpu.VMEM((32, CH, 128), bf16),
            pltpu.VMEM((32, 128, CH), bf16),
            pltpu.VMEM((2 * CH, CH), f32),
            pltpu.VMEM((2 * CH, CH), f32),
            pltpu.VMEM((2 * CH, CH), bf16),
            pltpu.VMEM((2 * CH, CH), bf16),
        ],
        cost_estimate=pl.CostEstimate(flops=20_000_000_000, bytes_accessed=4_000_000, transcendentals=26_000_000),
        name="stick_attention",
    )(table, off, q, u, *kvs)


def fetch(own, other, x_all, sems):
    copies = []
    for h, pieces in enumerate((own, other)):
        at = 0
        for k, piece in enumerate(pieces):
            rows = piece.shape[0]
            to = x_all.at[at // CH, pl.ds(at % CH, rows), pl.ds(h * 1024, 1024)]
            copy = pltpu.make_async_copy(piece, to, sems.at[h, k])
            copy.start()
            copies.append(copy)
            at += rows
    return copies


def project_rows(w_copies, copies, one, x_all, sems, w_ref, q_ref, kv_ref):
    for copy in w_copies:
        copy.wait()
    halves = len(copies) // 2

    def chunk(n):
        out = jnp.dot(x_all[n], w_ref[...], preferred_element_type=f32).astype(bf16)
        q_ref[n] = out[:, :128]
        kv_ref[n] = out[:, 128:]

    def whole(n, carry):
        for h in range(2):
            pltpu.make_async_copy(one, x_all.at[n, :, pl.ds(h * 1024, 1024)], sems.at[h, n]).wait()
        chunk(n)
        return carry

    lax.fori_loop(0, 7, whole, 0)
    for k in (7, 8, halves + 7, halves + 8):
        copies[k].wait()
    chunk(7)


def fetch_weights(place, pieces, columns, w_all, sems):
    copies = []
    for d, piece in enumerate(pieces):
        at = lax.rem(place[1] - d - 2 * place[2] + 8, 4)
        to = w_all.at[pl.ds(pl.multiple_of(at * 512, 512), 512), :]
        copy = pltpu.make_async_copy(piece.at[:, columns], to, sems.at[d])
        copy.start()
        copies.append(copy)
    return copies


def project_kernel(place, *refs):
    weights, x, (q_ref, kv_ref, w_all, x_all, sems, w_sems) = refs[:4], refs[4:-6], refs[-6:]
    half = len(x) // 2
    w_copies = fetch_weights(place, weights, pl.ds(0, 256), w_all, w_sems)
    copies = fetch(x[:half], x[half:], x_all, sems)
    project_rows(w_copies, copies, x[0], x_all, sems, w_all, q_ref, kv_ref)


def stick_project(place, weights, own, other):
    vmem = pl.BlockSpec(memory_space=pltpu.VMEM)
    anywhere = pl.BlockSpec(memory_space=pl.ANY)
    shape = jax.ShapeDtypeStruct((8, CH, 128), bf16)
    return pl.pallas_call(
        project_kernel,
        out_shape=(shape, shape),
        in_specs=[pl.BlockSpec(memory_space=pltpu.SMEM)] + [anywhere] * (4 + len(own) + len(other)),
        out_specs=(vmem, vmem),
        scratch_shapes=[
            pltpu.VMEM((2048, 256), bf16),
            pltpu.VMEM((8, CH, 2048), bf16),
            pltpu.SemaphoreType.DMA((2, len(own))),
            pltpu.SemaphoreType.DMA((4,)),
        ],
        cost_estimate=pl.CostEstimate(flops=2_200_000_000, bytes_accessed=10_000_000, transcendentals=0),
        name="stick_project",
    )(place, *weights, *own, *other)


def mm(a, b, dims=(((1,), (0,)), ((), ()))):
    return lax.dot_general(a.astype(bf16), b.astype(bf16), dims, preferred_element_type=f32)


def silu(u):
    return u * jax.nn.sigmoid(u)


def unit(u):
    return u * lax.rsqrt(jnp.sum(u * u, axis=-1, keepdims=True) + EPS)


def delta_kernel(place, scale_ref, bias_ref, decay_ref, write_ref, *refs):
    shifts, weights, own, other = refs[:4], refs[4:8], refs[8:12], refs[12:16]
    qf_ref, of_ref, end_ref, x_all, w_all, side_w, proj_all, maps, addend, rows_all, sems, w_sems = refs[16:]
    y, tp = place[0], place[2]
    w_copies = fetch_weights(place, weights, pl.ds(256, 384), w_all, w_sems)
    fetch(own, other, x_all, sems)
    minus_scale = -jnp.exp(jnp.full((CH, 1), scale_ref[y], f32))
    bias = bias_ref[y]
    for h in range(2):
        at = pl.ds(pl.multiple_of((tp if h == 0 else 1 - tp) * 1024, 1024), 1024)
        side_w[:, h * 1024 : h * 1024 + 1024] = jnp.concatenate([decay_ref[:, at], write_ref[:, at]], axis=0)
    lanes = lax.broadcasted_iota(jnp.int32, (CH, 128), 1)
    for d in range(4):
        proj_all[lax.rem(y - d + 4, 4), :, 384:] = jnp.transpose(jnp.broadcast_to(shifts[d][pl.ds(y, 1), :], (128, CH)))
    for copy in w_copies:
        copy.wait()
    narrow = lax.broadcasted_iota(jnp.int32, (CH, 8), 1)

    def project(d, carry):
        for h in range(2):
            pltpu.make_async_copy(own[0], x_all.at[d, :, pl.ds(h * 1024, 1024)], sems.at[h, d]).wait()
        x = x_all[d]
        at = lax.rem(y - d + 4, 4)
        proj_all[at, :, :384] = jnp.dot(x, w_all[...], preferred_element_type=f32)
        pre = lax.dot_general(x, side_w[...], NT, preferred_element_type=f32)
        decay_pre = jnp.sum(jnp.where(narrow == y, pre, 0.0), axis=1, keepdims=True)
        write_pre = jnp.sum(jnp.where(narrow == y + 4, pre, 0.0), axis=1, keepdims=True)
        proj_all[at, :, 384:] = jnp.where(lanes == 0, decay_pre, jnp.where(lanes == 1, write_pre, proj_all[at, :, 384:]))
        return carry

    lax.fori_loop(0, 4, project, 0)
    span = (CH, CH)
    row = lax.broadcasted_iota(jnp.int32, span, 0)
    col = lax.broadcasted_iota(jnp.int32, span, 1)
    same = (row // 64) == (col // 64)
    inclusive = jnp.logical_and(same, col <= row)
    strict = jnp.logical_and(same, col < row)
    sums = jnp.concatenate([jnp.where(inclusive, 1.0, 0.0), jnp.where(same, 1.0, 0.0)], axis=0)
    eye = jnp.where(row == col, 1.0, 0.0)
    wide = lax.broadcasted_iota(jnp.int32, (128, CH), 1) // 64
    small_eye = jnp.where(
        lax.broadcasted_iota(jnp.int32, (128, 128), 0) == lax.broadcasted_iota(jnp.int32, (128, 128), 1), 1.0, 0.0
    )

    def blocks(m, carry):
        tiles = range(2)
        cum, tot, q, k, v, beta = [], [], [], [], [], []
        for t in tiles:
            proj = proj_all[2 * m + t]
            dq, dk, dv = (proj[:, 128 * n : 128 * n + 128].astype(bf16).astype(f32) for n in range(3))
            pre = proj[:, 384:385]
            softplus = jnp.maximum(pre, 0.0) + jnp.log1p(jnp.exp(-jnp.abs(pre)))
            g = minus_scale * softplus + proj[:, 386:387]
            beta.append(jax.nn.sigmoid(proj[:, 385:386] + bias))
            q.append(unit(silu(dq)) * 128**-0.5)
            k.append(unit(silu(dk)))
            v.append(silu(dv))
            g1 = g.astype(bf16).astype(f32)
            g2 = (g - g1).astype(bf16).astype(f32)
            g3 = g - g1 - g2
            parts = jnp.where(lanes == 0, g1, jnp.where(lanes == 1, g2, jnp.where(lanes == 2, g3, 0.0)))
            s = mm(sums, parts)
            s = jnp.broadcast_to(s[:, 0:1] + s[:, 1:2] + s[:, 2:3], (2 * CH, 128))
            cum.append(s[:CH])
            tot.append(s[CH:])
        table = []
        for t in tiles:
            across = jnp.transpose(cum[t])[0:1, :]
            spread = cum[t][:, 0:1] - across
            table.append(jnp.where(inclusive, jnp.exp(jnp.where(inclusive, spread, 0.0)), 0.0))
        keys_beta = [k[t] * beta[t] for t in tiles]
        power = [jnp.where(strict, mm(keys_beta[t], k[t], NT) * table[t], 0.0) for t in tiles]
        inside = [mm(q[t], k[t], NT) * table[t] for t in tiles]
        inverse = [eye - power[t] for t in tiles]
        for _ in range(5):
            power = [mm(power[t], power[t]) for t in tiles]
            inverse = [inverse[t] + mm(inverse[t], power[t]) for t in tiles]
        growth = [jnp.exp(cum[t]) for t in tiles]
        both = [
            mm(inverse[t], jnp.concatenate([keys_beta[t] * growth[t], v[t] * beta[t]], axis=1)) for t in tiles
        ]
        seen = [mm(inside[t], both[t]) for t in tiles]
        for t in tiles:
            n0 = 4 * (2 * m + t)
            reach = q[t] * growth[t] - seen[t][:, :128]
            damped = jnp.transpose(k[t] * jnp.exp(tot[t] - cum[t]))
            moved = mm(jnp.concatenate([jnp.where(wide == b, damped, 0.0) for b in range(4)], axis=0), both[t])
            for b in range(4):
                decay = jnp.exp(tot[t][b * 64 : b * 64 + 1, :])
                piece = moved[b * 128 : b * 128 + 128]
                maps[n0 + b, :64] = reach[b * 64 : b * 64 + 64].astype(bf16)
                maps[n0 + b, 64:] = (small_eye * decay - piece[:, :128]).astype(bf16)
                addend[n0 + b, :64] = seen[t][b * 64 : b * 64 + 64, 128:]
                addend[n0 + b, 64:] = piece[:, 128:]
        return carry

    lax.fori_loop(0, 2, blocks, 0)
    rows_all[...] = jnp.concatenate([small_eye, jnp.zeros((128, 128), f32)], axis=1)

    def chain(n, carry):
        moved = jnp.dot(maps[n], rows_all[...].astype(bf16), preferred_element_type=f32)
        after = moved[:, 128:] + addend[n]
        at = pl.ds(pl.multiple_of(n * 64, 64), 64)
        qf_ref[at, :] = moved[:64, :128]
        of_ref[at, :] = after[:64]
        rows_all[...] = jnp.concatenate([moved[64:, :128], after[64:]], axis=1)
        return carry

    lax.fori_loop(0, 16, chain, 0)
    end_ref[...] = rows_all[...].astype(bf16)


def delta_local(place, scale, bias, decay_w, write_w, weights, own, other, shifts):
    smem = pl.BlockSpec(memory_space=pltpu.SMEM)
    vmem = pl.BlockSpec(memory_space=pltpu.VMEM)
    return pl.pallas_call(
        delta_kernel,
        out_shape=(
            jax.ShapeDtypeStruct((1024, 128), f32),
            jax.ShapeDtypeStruct((1024, 128), f32),
            jax.ShapeDtypeStruct((128, 256), bf16),
        ),
        in_specs=[smem] * 3 + [vmem] * 6 + [pl.BlockSpec(memory_space=pl.ANY)] * 12,
        out_specs=(vmem,) * 3,
        scratch_shapes=[
            pltpu.VMEM((4, CH, 2048), bf16),
            pltpu.VMEM((2048, 384), bf16),
            pltpu.VMEM((8, 2048), bf16),
            pltpu.VMEM((4, CH, 512), f32),
            pltpu.VMEM((16, 192, 128), bf16),
            pltpu.VMEM((16, 192, 128), f32),
            pltpu.VMEM((128, 256), f32),
            pltpu.SemaphoreType.DMA((2, 4)),
            pltpu.SemaphoreType.DMA((4,)),
        ],
        cost_estimate=pl.CostEstimate(flops=12_000_000_000, bytes_accessed=8_000_000, transcendentals=1_000_000),
        name="delta_local",
    )(place, scale, bias, decay_w, write_w, *shifts, *weights, *own, *other)


def finish_kernel(gain_ref, qf_ref, of_ref, *refs):
    maps, o_ref = refs[:-1], refs[-1]
    state = jnp.zeros((128, 128), f32)
    for ref in maps:
        state = mm(ref[:, :128], state) + ref[:, 128:].astype(f32)
    for t in range(4):
        rows = slice(t * CH, (t + 1) * CH)
        o = mm(qf_ref[rows, :], state) + of_ref[rows, :]
        o = o * lax.rsqrt(jnp.mean(o * o, axis=-1, keepdims=True) + EPS) * gain_ref[...]
        o_ref[rows, :] = o.astype(bf16)


def delta_finish(gain, qf, of, maps):
    vmem = pl.BlockSpec(memory_space=pltpu.VMEM)
    return pl.pallas_call(
        finish_kernel,
        out_shape=jax.ShapeDtypeStruct((1024, 128), bf16),
        in_specs=[vmem] * (3 + len(maps)),
        out_specs=vmem,
        cost_estimate=pl.CostEstimate(flops=1_000_000_000, bytes_accessed=2_000_000, transcendentals=2_000),
        name="delta_finish",
    )(gain, qf, of, *maps)


def ring(axis, size, step):
    return functools.partial(lax.ppermute, axis_name=axis, perm=[(i, (i + step) % size) for i in range(size)])


def on_device(
    hidden_in,
    sb_query_w,
    sb_key_w,
    sb_value_w,
    sb_offset,
    delta_query_w,
    delta_key_w,
    delta_value_w,
    decay_w,
    write_w,
    write_bias,
    decay_log_scale,
    decay_shift,
    head_gain,
    sb_out_w,
    delta_out_w,
):
    z, y, fs, tp = lax.axis_index(Z), lax.axis_index("y"), lax.axis_index("fs"), lax.axis_index("tp")
    x = hidden_in.reshape(256, 1024)

    across = functools.partial(lax.ppermute, axis_name="tp", perm=[(0, 1), (1, 0)])
    swap = lambda v: across(v)
    right, left = ring(Z, 8, 1), ring(Z, 8, 7)
    around = lambda axis, v: [v] + [ring(axis, 4, d)(v) for d in (1, 2, 3)]
    pick = lambda w, at, n: lax.dynamic_slice_in_dim(w, at, n, 1)
    item = lambda v, at: lax.dynamic_index_in_dim(v, at, 0, keepdims=False)

    mine = jnp.concatenate(
        [pick(sb_query_w, z * 64, 64), jnp.zeros((512, 64), bf16), pick(sb_key_w, z * 64, 64), pick(sb_value_w, z * 64, 64)]
        + [pick(w, y * 128, 128) for w in (delta_query_w, delta_key_w, delta_value_w)],
        axis=1,
    )
    r1, l1 = right(x), left(x)
    at_y = around("y", x)
    weights = around("fs", mine)
    r2, l2 = right(r1), left(l1)
    r3, l3 = right(r2), left(l2)
    r4, l4 = right(r3[:128]), left(l3[128:])
    other_y = [swap(v) for v in at_y]
    other_r = [swap(v) for v in (r1, r2, r3, r4)]
    other_l = [swap(v) for v in (l1, l2, l3, l4)]
    shifts = around("y", decay_shift.reshape(4, 256))

    place = jnp.stack([y, fs, tp]).astype(jnp.int32)
    q, kv = stick_project(
        place,
        weights,
        [x, r1, l1, r2, l2, r3, l3, r4, l4],
        [other_y[0]] + [v for pair in zip(other_r, other_l) for v in pair],
    )
    kvs = around("y", kv)
    qf, of, end = delta_local(
        place, decay_log_scale, write_bias, decay_w.T, write_w.T, weights, at_y, other_y, shifts
    )
    ends = [
        functools.partial(lax.ppermute, axis_name=Z, perm=[(i, i + d) for i in range(8 - d)])(end)
        for d in range(7, 0, -1)
    ]
    dm = delta_finish(head_gain.reshape(1, 128), qf, of, ends)
    dm = lax.all_to_all(dm.reshape(8, 128, 128), ("y", "tp"), 0, 0, tiled=True)
    outs_other = [swap(sb_out_w), swap(delta_out_w)]

    u = jnp.asarray(np.tril(np.ones((CH, CH), np.float32), -1), bf16)
    sb = stick_attention(item(jnp.asarray(work_list()), 4 * z + y), sb_offset, q, u, kvs)
    sb = lax.all_to_all(sb, (*Z, "tp"), 0, 0, tiled=True)

    sb = sb.reshape(8, 2, 64, 2, 64).transpose(1, 3, 2, 0, 4).reshape(2, 128, 512)
    dm = dm.reshape(4, 2, 128, 128).transpose(1, 2, 0, 3).reshape(2, 128, 512)

    def out_rows(rows, own_w, other_w):
        return jnp.dot(item(rows, tp), own_w, preferred_element_type=f32) + jnp.dot(
            item(rows, 1 - tp), other_w, preferred_element_type=f32
        )

    out = out_rows(dm, delta_out_w, outs_other[1])
    out = out + out_rows(sb, sb_out_w, outs_other[0])
    return out.astype(bf16).reshape(1, 128, 2048)


def solution(mesh):
    finer = Mesh(mesh.devices.reshape(2, 4, 4, mesh.shape["fs"], mesh.shape["tp"]), AXES)
    sp = ("zh", "zl", "y")
    return jax.shard_map(
        on_device,
        mesh=finer,
        in_specs=(
            P("fs", sp, "tp"),
            P("fs", "tp"),
            P("fs", "tp"),
            P("fs", "tp"),
            P("tp"),
            P("fs", "tp"),
            P("fs", "tp"),
            P("fs", "tp"),
            P(None, "tp"),
            P(None, "tp"),
            P("tp"),
            P("tp"),
            P("fs", "tp", sp),
            P(),
            P("tp", None),
            P("tp", None),
        ),
        out_specs=P("fs", (*sp, "tp"), None),
        check_vma=False,
    )
```

profile of v0, /device:TPU:25, one launch (start us, length us, event | category | flops | bytes accessed | tf_op | source)
XLA Modules:
  0.0 220.0 jit_solution(10180692187829303974)
XLA Ops:
  1.6 4.0 %collective-permute-start.22 = (bf16[256,1024]{1,0:T(8,128)(2,1)}, bf16[256,1024]{1,0:T(8,128)(2,1)S(1)}, u32[]{:S(2)}, u32[]{:S(2)}) collective-permute-start(bf16[256,1024]{1,0:T(8,128)(2,1)} %bitcast.41), channel_id=1, source_target_pairs={{0,224},{32,0},{64,32},{96,64},{128,96},{160,128},{192,160},{224,1... | collective-permute-start | bytes 1572872 | tf_op jit(solution)/shard_map/ppermute | solution.py:447
  12.7 2.6 %collective-permute-done.2.refs_3_ = f32[4,256]{1,0:T(4,128)S(1)} collective-permute-done((f32[4,256]{1,0:T(4,128)}, f32[4,256]{1,0:T(4,128)S(1)}, u32[]{:S(2)}, u32[]{:S(2)}) %collective-permute-start.2) | collective-permute-done | bytes 4128 | tf_op jit(solution)/shard_map/ppermute | solution.py:438
  24.6 4.2 %collective-permute-done.7.refs_10_ = bf16[256,1024]{1,0:T(8,128)(2,1)} collective-permute-done((bf16[256,1024]{1,0:T(8,128)(2,1)}, bf16[256,1024]{1,0:T(8,128)(2,1)}, u32[]{:S(2)}, u32[]{:S(2)}) %collective-permute-start.7) | collective-permute-done | bytes 524320 | tf_op jit(solution)/shard_map/ppermute | solution.py:438
  28.8 2.7 %collective-permute-start.4 = (bf16[512,640]{1,0:T(8,128)(2,1)S(1)}, bf16[512,640]{1,0:T(8,128)(2,1)S(1)}, u32[]{:S(2)}, u32[]{:S(2)}) collective-permute-start(bf16[512,640]{1,0:T(8,128)(2,1)S(1)} %concatenate.3.refs_4_.refs_0_), channel_id=1, source_target_pairs={{0,4},{2,6},{4,0},{6,2},{1,5},{3,7},{5,1},{7,3},{8,12},{10,14},{12... | collective-permute-start | bytes 1966088 | tf_op jit(solution)/shard_map/ppermute | solution.py:438
  31.6 10.7 %collective-permute-done.8.refs_11_ = bf16[256,1024]{1,0:T(8,128)(2,1)} collective-permute-done((bf16[256,1024]{1,0:T(8,128)(2,1)}, bf16[256,1024]{1,0:T(8,128)(2,1)}, u32[]{:S(2)}, u32[]{:S(2)}) %collective-permute-start.8) | collective-permute-done | bytes 524320 | tf_op jit(solution)/shard_map/ppermute | solution.py:438
  45.5 2.9 %collective-permute-start.26 = (bf16[256,1024]{1,0:T(8,128)(2,1)S(1)}, bf16[256,1024]{1,0:T(8,128)(2,1)S(1)}, u32[]{:S(2)}, u32[]{:S(2)}) collective-permute-start(bf16[256,1024]{1,0:T(8,128)(2,1)S(1)} %collective-permute-done.24.refs_8_), channel_id=1, source_target_pairs={{0,224},{32,0},{64,32},{96,64},{128,96},{160,128},{192,160},{224,1... | collective-permute-start | bytes 1572872 | tf_op jit(solution)/shard_map/ppermute | solution.py:451
  48.4 3.2 %collective-permute-done.4.refs_6_.refs_2_ = bf16[512,640]{1,0:T(8,128)(2,1)S(1)} collective-permute-done((bf16[512,640]{1,0:T(8,128)(2,1)S(1)}, bf16[512,640]{1,0:T(8,128)(2,1)S(1)}, u32[]{:S(2)}, u32[]{:S(2)}) %collective-permute-start.4) | collective-permute-done | bytes 655392 | tf_op jit(solution)/shard_map/ppermute | solution.py:438
  54.1 7.6 %collective-permute-done.5.refs_7_.refs_3_ = bf16[512,640]{1,0:T(8,128)(2,1)S(1)} collective-permute-done((bf16[512,640]{1,0:T(8,128)(2,1)S(1)}, bf16[512,640]{1,0:T(8,128)(2,1)S(1)}, u32[]{:S(2)}, u32[]{:S(2)}) %collective-permute-start.5) | collective-permute-done | bytes 655392 | tf_op jit(solution)/shard_map/ppermute | solution.py:438
  65.6 2.7 %collective-permute-start.28 = (bf16[128,1024]{1,0:T(8,128)(2,1)}, bf16[128,1024]{1,0:T(8,128)(2,1)}, u32[]{:S(2)}, u32[]{:S(2)}) collective-permute-start(bf16[128,1024]{1,0:T(8,128)(2,1)} %slice.9), channel_id=1, source_target_pairs={{0,224},{32,0},{64,32},{96,64},{128,96},{160,128},{192,160},{224,1... | collective-permute-start | bytes 786440 | tf_op jit(solution)/shard_map/ppermute | solution.py:452
  70.2 4.4 %collective-permute-done.27.refs_11_ = bf16[128,1024]{1,0:T(8,128)(2,1)} collective-permute-done((bf16[128,1024]{1,0:T(8,128)(2,1)}, bf16[128,1024]{1,0:T(8,128)(2,1)}, u32[]{:S(2)}, u32[]{:S(2)}) %collective-permute-start.27) | collective-permute-done | bytes 262176 | tf_op jit(solution)/shard_map/ppermute | solution.py:452
  75.8 17.8 %delta_local.1 = (f32[1024,128]{1,0:T(8,128)}, f32[1024,128]{1,0:T(8,128)}, bf16[128,256]{1,0:T(8,128)(2,1)}) custom-call(s32[3]{0:T(128)} %pad_add_fusion.place, f32[4]{0:T(128)} %scale_ref.1, f32[4]{0:T(128)} %bias_ref.1, bf16[4,2048]{1,0:T(4,128)(2,1)} %bitcast.49, bf16[4,2048]{1,0:T(4,128)(2,1)} %bitcast.50, f32[4,256]{1,0:T(4,128)} %bitcast.54, ...), custom_call_target="tpu_custom_call" | custom-call | flops 12000000000 | bytes 8000000 | tf_op jit(solution)/shard_map/delta_local/pallas_call | solution.py:361
  93.7 4.7 %collective-permute-start.13 = (bf16[128,256]{1,0:T(8,128)(2,1)}, bf16[128,256]{1,0:T(8,128)(2,1)S(1)}, u32[]{:S(2)}, u32[]{:S(2)}) collective-permute-start(bf16[128,256]{1,0:T(8,128)(2,1)} %get-tuple-element.12), channel_id=1, source_target_pairs={{0,224},{1,225},{2,226},{3,227},{4,228},{5,229},{6,230},{7,231},{8... | collective-permute-start | bytes 196616 | tf_op jit(solution)/shard_map/ppermute | solution.py:470
  98.5 9.1 %stick_project.1 = (bf16[8,256,128]{2,1,0:T(8,128)(2,1)}, bf16[8,256,128]{2,1,0:T(8,128)(2,1)}) custom-call(s32[3]{0:T(128)} %pad_add_fusion.place, bf16[512,640]{1,0:T(8,128)(2,1)} %copy-done.1, bf16[512,640]{1,0:T(8,128)(2,1)} %copy-done.5, bf16[512,640]{1,0:T(8,128)(2,1)} %copy-done.6, bf16[512,640]{1,0:T(8,128)(2,1)} %copy-done.7, ...), custom_call_target="tpu_custom_call" | custom-call | flops 2200000000 | bytes 10000000 | tf_op jit(solution)/shard_map/stick_project/pallas_call | solution.py:218
  107.6 6.1 %collective-permute-start.37 = (bf16[8,256,128]{2,1,0:T(8,128)(2,1)}, bf16[8,256,128]{2,1,0:T(8,128)(2,1)}, u32[]{:S(2)}, u32[]{:S(2)}) collective-permute-start(bf16[8,256,128]{2,1,0:T(8,128)(2,1)} %get-tuple-element.14.refs_0_), channel_id=1, source_target_pairs={{0,8},{8,16},{16,24},{24,0},{1,9},{9,17},{17,25},{25,1},{2,10},{10... | collective-permute-start | bytes 1572872 | tf_op jit(solution)/shard_map/ppermute | solution.py:438
  118.3 5.8 %collective-permute-done.15.refs_2_ = bf16[128,256]{1,0:T(8,128)(2,1)S(1)} collective-permute-done((bf16[128,256]{1,0:T(8,128)(2,1)S(1)}, bf16[128,256]{1,0:T(8,128)(2,1)S(1)}, u32[]{:S(2)}, u32[]{:S(2)}) %collective-permute-start.15) | collective-permute-done | bytes 65568 | tf_op jit(solution)/shard_map/ppermute | solution.py:470
  124.0 4.0 %collective-permute-start.17 = (bf16[128,256]{1,0:T(8,128)(2,1)S(1)}, bf16[128,256]{1,0:T(8,128)(2,1)S(1)}, u32[]{:S(2)}, u32[]{:S(2)}) collective-permute-start(bf16[128,256]{1,0:T(8,128)(2,1)S(1)} %copy-done.12), channel_id=1, source_target_pairs={{0,96},{32,128},{64,160},{96,192},{128,224},{1,97},{33,129},{65,16... | collective-permute-start | bytes 196616 | tf_op jit(solution)/shard_map/ppermute | solution.py:470
  128.1 6.2 %collective-permute-start.18 = (bf16[128,256]{1,0:T(8,128)(2,1)S(1)}, bf16[128,256]{1,0:T(8,128)(2,1)S(1)}, u32[]{:S(2)}, u32[]{:S(2)}) collective-permute-start(bf16[128,256]{1,0:T(8,128)(2,1)S(1)} %copy-done.12), channel_id=1, source_target_pairs={{0,64},{32,96},{64,128},{96,160},{128,192},{160,224},{1,65},{33,97... | collective-permute-start | bytes 196616 | tf_op jit(solution)/shard_map/ppermute | solution.py:470
  137.5 3.4 %delta_finish.1 = bf16[1024,128]{1,0:T(8,128)(2,1)} custom-call(f32[1,128]{1,0:T(1,128)} %bitcast.55, f32[1024,128]{1,0:T(8,128)} %get-tuple-element.10.qf_ref, f32[1024,128]{1,0:T(8,128)} %get-tuple-element.11.of_ref, bf16[128,256]{1,0:T(8,128)(2,1)} %copy-done.13, bf16[128,256]{1,0:T(8,128)(2,1)} %copy-done.14, bf16[128,256]{1,0:T(8,128)(2,1)} %copy-done.15, ...), custom_call_target="tpu_custom_call" | custom-call | flops 1000000000 | bytes 2000000 | tf_op jit(solution)/shard_map/delta_finish/pallas_call | solution.py:400
  141.0 9.8 %all-to-all-start = ((bf16[8,128,128]{2,1,0:T(8,128)(2,1)}), bf16[8,128,128]{2,1,0:T(8,128)(2,1)S(1)}, u32[]{:S(2)}, u32[]{:S(2)}) async-start(bf16[8,128,128]{2,1,0:T(8,128)(2,1)} %bitcast.48), calls=%async_computation | async-start | bytes 524288 | tf_op jit(solution)/shard_map/all_to_all | solution.py:474
  152.6 3.0 %all-to-all-done = bf16[8,128,128]{2,1,0:T(8,128)(2,1)S(1)} async-done(((bf16[8,128,128]{2,1,0:T(8,128)(2,1)}), bf16[8,128,128]{2,1,0:T(8,128)(2,1)S(1)}, u32[]{:S(2)}, u32[]{:S(2)}) %all-to-all-start) | async-done | bytes 262176 | tf_op jit(solution)/shard_map/all_to_all | solution.py:474
  155.8 34.6 %stick_attention.1 = bf16[16,64,128]{2,1,0:T(8,128)(2,1)} custom-call(s32[384]{0:T(512)} %fusion.17.table, f32[8]{0:T(128)} %off_ref.1, bf16[8,256,128]{2,1,0:T(8,128)(2,1)} %get-tuple-element.13.q, bf16[256,256]{1,0:T(8,128)(2,1)} %constant.55.clone.u_ref, bf16[8,256,128]{2,1,0:T(8,128)(2,1)} %get-tuple-element.14.refs_0_, ...), custom_call_target="tpu_custom_call" | custom-call | flops 20000000000 | bytes 4000000 | tf_op jit(solution)/shard_map/stick_attention/pallas_call | solution.py:139
  190.4 12.2 %all-to-all-start.1 = ((bf16[16,64,128]{2,1,0:T(8,128)(2,1)}), bf16[16,64,128]{2,1,0:T(8,128)(2,1)S(1)}, u32[]{:S(2)}, u32[]{:S(2)}) async-start(bf16[16,64,128]{2,1,0:T(8,128)(2,1)} %stick_attention.1), calls=%async_computation.1 | async-start | bytes 524288 | tf_op jit(solution)/shard_map/all_to_all | solution.py:479
  205.2 9.0 %all-to-all-done.1 = bf16[16,64,128]{2,1,0:T(8,128)(2,1)S(1)} async-done(((bf16[16,64,128]{2,1,0:T(8,128)(2,1)}), bf16[16,64,128]{2,1,0:T(8,128)(2,1)S(1)}, u32[]{:S(2)}, u32[]{:S(2)}) %all-to-all-start.1) | async-done | bytes 262176 | tf_op jit(solution)/shard_map/all_to_all | solution.py:479
  217.1 2.9 %fusion.2 = bf16[1,128,2048]{2,1,0:T(8,128)(2,1)} fusion(f32[128,2048]{1,0:T(8,128)S(1)} %convolution_add_fusion.1, f32[128,2048]{1,0:T(8,128)S(1)} %fusion.4, bf16[512,2048]{1,0:T(8,128)(2,1)} %collective-permute-done.40, bf16[2,128,512]{2,1,0:T(8,128)(2,1)S(1)} %reshape.34, s32[]{:T(128)S(6)} %select_n.26), kind=kOutput, calls=%fused_computation.4 | convolution fusion | flops 269221888 | bytes 4849668 | tf_op jit(solution)/shard_map/dot_general | solution.py:485
  (130 shorter events, 45.8 us)
Async XLA Ops:
  0.0 17.5 %collective-permute-start.21 = (bf16[256,1024]{1,0:T(8,128)(2,1)}, bf16[256,1024]{1,0:T(8,128)(2,1)}, u32[]{:S(2)}, u32[]{:S(2)}) collective-permute-start(bf16[256,1024]{1,0:T(8,128)(2,1)} %bitcast.40), channel_id=1, source_target_pairs={{0,32},{32,64},{64,96},{96,128},{128,160},{160,192},{192,224},{224... | collective-permute-start | bytes 1572872 | tf_op jit(solution)/shard_map/ppermute | solution.py:447
  1.6 18.9 %collective-permute-start.22 = (bf16[256,1024]{1,0:T(8,128)(2,1)}, bf16[256,1024]{1,0:T(8,128)(2,1)S(1)}, u32[]{:S(2)}, u32[]{:S(2)}) collective-permute-start(bf16[256,1024]{1,0:T(8,128)(2,1)} %bitcast.41), channel_id=1, source_target_pairs={{0,224},{32,0},{64,32},{96,64},{128,96},{160,128},{192,160},{224,1... | collective-permute-start | bytes 1572872 | tf_op jit(solution)/shard_map/ppermute | solution.py:447
  17.5 24.7 %collective-permute-start.8 = (bf16[256,1024]{1,0:T(8,128)(2,1)}, bf16[256,1024]{1,0:T(8,128)(2,1)}, u32[]{:S(2)}, u32[]{:S(2)}) collective-permute-start(bf16[256,1024]{1,0:T(8,128)(2,1)} %bitcast.45), channel_id=1, source_target_pairs={{0,24},{8,0},{16,8},{24,16},{1,25},{9,1},{17,9},{25,17},{2,26},{10... | collective-permute-start | bytes 1572872 | tf_op jit(solution)/shard_map/ppermute | solution.py:438
  20.6 24.1 %collective-permute-start.3 = (bf16[512,640]{1,0:T(8,128)(2,1)S(1)}, bf16[512,640]{1,0:T(8,128)(2,1)S(1)}, u32[]{:S(2)}, u32[]{:S(2)}) collective-permute-start(bf16[512,640]{1,0:T(8,128)(2,1)S(1)} %concatenate.3.refs_4_.refs_0_), channel_id=1, source_target_pairs={{0,2},{2,4},{4,6},{6,0},{1,3},{3,5},{5,7},{7,1},{8,10},{10,12},{12... | collective-permute-start | bytes 1966088 | tf_op jit(solution)/shard_map/ppermute | solution.py:438
  21.9 23.6 %collective-permute-start.23 = (bf16[256,1024]{1,0:T(8,128)(2,1)}, bf16[256,1024]{1,0:T(8,128)(2,1)}, u32[]{:S(2)}, u32[]{:S(2)}) collective-permute-start(bf16[256,1024]{1,0:T(8,128)(2,1)} %collective-permute-done.21.refs_5_), channel_id=1, source_target_pairs={{0,32},{32,64},{64,96},{96,128},{128,160},{160,192},{192,224},{224... | collective-permute-start | bytes 1572872 | tf_op jit(solution)/shard_map/ppermute | solution.py:450
  22.5 23.0 %collective-permute-start.24 = (bf16[256,1024]{1,0:T(8,128)(2,1)S(1)}, bf16[256,1024]{1,0:T(8,128)(2,1)S(1)}, u32[]{:S(2)}, u32[]{:S(2)}) collective-permute-start(bf16[256,1024]{1,0:T(8,128)(2,1)S(1)} %collective-permute-done.22.refs_6_), channel_id=1, source_target_pairs={{0,224},{32,0},{64,32},{96,64},{128,96},{160,128},{192,160},{224,1... | collective-permute-start | bytes 1572872 | tf_op jit(solution)/shard_map/ppermute | solution.py:450
  28.8 22.8 %collective-permute-start.4 = (bf16[512,640]{1,0:T(8,128)(2,1)S(1)}, bf16[512,640]{1,0:T(8,128)(2,1)S(1)}, u32[]{:S(2)}, u32[]{:S(2)}) collective-permute-start(bf16[512,640]{1,0:T(8,128)(2,1)S(1)} %concatenate.3.refs_4_.refs_0_), channel_id=1, source_target_pairs={{0,4},{2,6},{4,0},{6,2},{1,5},{3,7},{5,1},{7,3},{8,12},{10,14},{12... | collective-permute-start | bytes 1966088 | tf_op jit(solution)/shard_map/ppermute | solution.py:438
  42.2 19.5 %collective-permute-start.5 = (bf16[512,640]{1,0:T(8,128)(2,1)S(1)}, bf16[512,640]{1,0:T(8,128)(2,1)S(1)}, u32[]{:S(2)}, u32[]{:S(2)}) collective-permute-start(bf16[512,640]{1,0:T(8,128)(2,1)S(1)} %concatenate.3.refs_4_.refs_0_), channel_id=1, source_target_pairs={{0,6},{2,0},{4,2},{6,4},{1,7},{3,1},{5,3},{7,5},{8,14},{10,8},{12,... | collective-permute-start | bytes 1966088 | tf_op jit(solution)/shard_map/ppermute | solution.py:438
  44.7 18.2 %collective-permute-start.29 = (bf16[256,1024]{1,0:T(8,128)(2,1)}, bf16[256,1024]{1,0:T(8,128)(2,1)S(1)}, u32[]{:S(2)}, u32[]{:S(2)}) collective-permute-start(bf16[256,1024]{1,0:T(8,128)(2,1)} %collective-permute-done.21.refs_5_), channel_id=1, source_target_pairs={{0,1},{1,0},{2,3},{3,2},{4,5},{5,4},{6,7},{7,6},{8,9},{9,8},{10,11... | collective-permute-start | bytes 1572872 | tf_op jit(solution)/shard_map/ppermute | solution.py:436
  45.5 17.6 %collective-permute-start.25 = (bf16[256,1024]{1,0:T(8,128)(2,1)}, bf16[256,1024]{1,0:T(8,128)(2,1)S(1)}, u32[]{:S(2)}, u32[]{:S(2)}) collective-permute-start(bf16[256,1024]{1,0:T(8,128)(2,1)} %collective-permute-done.23.refs_7_), channel_id=1, source_target_pairs={{0,32},{32,64},{64,96},{96,128},{128,160},{160,192},{192,224},{224... | collective-permute-start | bytes 1572872 | tf_op jit(solution)/shard_map/ppermute | solution.py:451
  45.5 17.9 %collective-permute-start.26 = (bf16[256,1024]{1,0:T(8,128)(2,1)S(1)}, bf16[256,1024]{1,0:T(8,128)(2,1)S(1)}, u32[]{:S(2)}, u32[]{:S(2)}) collective-permute-start(bf16[256,1024]{1,0:T(8,128)(2,1)S(1)} %collective-permute-done.24.refs_8_), channel_id=1, source_target_pairs={{0,224},{32,0},{64,32},{96,64},{128,96},{160,128},{192,160},{224,1... | collective-permute-start | bytes 1572872 | tf_op jit(solution)/shard_map/ppermute | solution.py:451
  68.8 24.9 %collective-permute-start.32 = (bf16[256,1024]{1,0:T(8,128)(2,1)}, bf16[256,1024]{1,0:T(8,128)(2,1)}, u32[]{:S(2)}, u32[]{:S(2)}) collective-permute-start(bf16[256,1024]{1,0:T(8,128)(2,1)} %copy-done.10), channel_id=1, source_target_pairs={{0,1},{1,0},{2,3},{3,2},{4,5},{5,4},{6,7},{7,6},{8,9},{9,8},{10,11... | collective-permute-start | bytes 1572872 | tf_op jit(solution)/shard_map/ppermute | solution.py:436
  69.7 28.7 %collective-permute-start.33 = (bf16[256,1024]{1,0:T(8,128)(2,1)S(1)}, bf16[256,1024]{1,0:T(8,128)(2,1)}, u32[]{:S(2)}, u32[]{:S(2)}) collective-permute-start(bf16[256,1024]{1,0:T(8,128)(2,1)S(1)} %collective-permute-done.25.refs_9_), channel_id=1, source_target_pairs={{0,1},{1,0},{2,3},{3,2},{4,5},{5,4},{6,7},{7,6},{8,9},{9,8},{10,11... | collective-permute-start | bytes 1572872 | tf_op jit(solution)/shard_map/ppermute | solution.py:436
  69.8 28.7 %collective-permute-start.34 = (bf16[256,1024]{1,0:T(8,128)(2,1)S(1)}, bf16[256,1024]{1,0:T(8,128)(2,1)}, u32[]{:S(2)}, u32[]{:S(2)}) collective-permute-start(bf16[256,1024]{1,0:T(8,128)(2,1)S(1)} %collective-permute-done.26.refs_10_), channel_id=1, source_target_pairs={{0,1},{1,0},{2,3},{3,2},{4,5},{5,4},{6,7},{7,6},{8,9},{9,8},{10,11... | collective-permute-start | bytes 1572872 | tf_op jit(solution)/shard_map/ppermute | solution.py:436
  74.6 23.8 %collective-permute-start.35 = (bf16[128,1024]{1,0:T(8,128)(2,1)}, bf16[128,1024]{1,0:T(8,128)(2,1)}, u32[]{:S(2)}, u32[]{:S(2)}) collective-permute-start(bf16[128,1024]{1,0:T(8,128)(2,1)} %collective-permute-done.27.refs_11_), channel_id=1, source_target_pairs={{0,1},{1,0},{2,3},{3,2},{4,5},{5,4},{6,7},{7,6},{8,9},{9,8},{10,11... | collective-permute-start | bytes 786440 | tf_op jit(solution)/shard_map/ppermute | solution.py:436
  75.8 22.6 %collective-permute-start.36 = (bf16[128,1024]{1,0:T(8,128)(2,1)}, bf16[128,1024]{1,0:T(8,128)(2,1)}, u32[]{:S(2)}, u32[]{:S(2)}) collective-permute-start(bf16[128,1024]{1,0:T(8,128)(2,1)} %collective-permute-done.28.refs_12_), channel_id=1, source_target_pairs={{0,1},{1,0},{2,3},{3,2},{4,5},{5,4},{6,7},{7,6},{8,9},{9,8},{10,11... | collective-permute-start | bytes 786440 | tf_op jit(solution)/shard_map/ppermute | solution.py:436
  93.7 21.9 %collective-permute-start.13 = (bf16[128,256]{1,0:T(8,128)(2,1)}, bf16[128,256]{1,0:T(8,128)(2,1)S(1)}, u32[]{:S(2)}, u32[]{:S(2)}) collective-permute-start(bf16[128,256]{1,0:T(8,128)(2,1)} %get-tuple-element.12), channel_id=1, source_target_pairs={{0,224},{1,225},{2,226},{3,227},{4,228},{5,229},{6,230},{7,231},{8... | collective-permute-start | bytes 196616 | tf_op jit(solution)/shard_map/ppermute | solution.py:470
  107.6 48.2 %collective-permute-start.37 = (bf16[8,256,128]{2,1,0:T(8,128)(2,1)}, bf16[8,256,128]{2,1,0:T(8,128)(2,1)}, u32[]{:S(2)}, u32[]{:S(2)}) collective-permute-start(bf16[8,256,128]{2,1,0:T(8,128)(2,1)} %get-tuple-element.14.refs_0_), channel_id=1, source_target_pairs={{0,8},{8,16},{16,24},{24,0},{1,9},{9,17},{17,25},{25,1},{2,10},{10... | collective-permute-start | bytes 1572872 | tf_op jit(solution)/shard_map/ppermute | solution.py:438
  113.6 42.1 %collective-permute-start.38 = (bf16[8,256,128]{2,1,0:T(8,128)(2,1)}, bf16[8,256,128]{2,1,0:T(8,128)(2,1)}, u32[]{:S(2)}, u32[]{:S(2)}) collective-permute-start(bf16[8,256,128]{2,1,0:T(8,128)(2,1)} %get-tuple-element.14.refs_0_), channel_id=1, source_target_pairs={{0,16},{8,24},{16,0},{24,8},{1,17},{9,25},{17,1},{25,9},{2,18},{10... | collective-permute-start | bytes 1572872 | tf_op jit(solution)/shard_map/ppermute | solution.py:438
  114.2 41.6 %collective-permute-start.39 = (bf16[8,256,128]{2,1,0:T(8,128)(2,1)}, bf16[8,256,128]{2,1,0:T(8,128)(2,1)}, u32[]{:S(2)}, u32[]{:S(2)}) collective-permute-start(bf16[8,256,128]{2,1,0:T(8,128)(2,1)} %get-tuple-element.14.refs_0_), channel_id=1, source_target_pairs={{0,24},{8,0},{16,8},{24,16},{1,25},{9,1},{17,9},{25,17},{2,26},{10... | collective-permute-start | bytes 1572872 | tf_op jit(solution)/shard_map/ppermute | solution.py:438
  141.0 14.6 %all-to-all-start = ((bf16[8,128,128]{2,1,0:T(8,128)(2,1)}), bf16[8,128,128]{2,1,0:T(8,128)(2,1)S(1)}, u32[]{:S(2)}, u32[]{:S(2)}) async-start(bf16[8,128,128]{2,1,0:T(8,128)(2,1)} %bitcast.48), calls=%async_computation | async-start | bytes 524288 | tf_op jit(solution)/shard_map/all_to_all | solution.py:474
  150.8 52.3 %collective-permute-start.20 = (bf16[512,2048]{1,0:T(8,128)(2,1)S(1)}, bf16[512,2048]{1,0:T(8,128)(2,1)}, u32[]{:S(2)}, u32[]{:S(2)}) collective-permute-start(bf16[512,2048]{1,0:T(8,128)(2,1)S(1)} %copy-done.2), channel_id=1, source_target_pairs={{0,1},{1,0},{2,3},{3,2},{4,5},{5,4},{6,7},{7,6},{8,9},{9,8},{10,11... | collective-permute-start | bytes 6291464 | tf_op jit(solution)/shard_map/ppermute | solution.py:436
  151.2 66.0 %collective-permute-start.40 = (bf16[512,2048]{1,0:T(8,128)(2,1)}, bf16[512,2048]{1,0:T(8,128)(2,1)}, u32[]{:S(2)}, u32[]{:S(2)}) collective-permute-start(bf16[512,2048]{1,0:T(8,128)(2,1)} %param.32), channel_id=1, source_target_pairs={{0,1},{1,0},{2,3},{3,2},{4,5},{5,4},{6,7},{7,6},{8,9},{9,8},{10,11... | collective-permute-start | bytes 6291464 | tf_op jit(solution)/shard_map/ppermute | solution.py:436
  190.4 23.8 %all-to-all-start.1 = ((bf16[16,64,128]{2,1,0:T(8,128)(2,1)}), bf16[16,64,128]{2,1,0:T(8,128)(2,1)S(1)}, u32[]{:S(2)}, u32[]{:S(2)}) async-start(bf16[16,64,128]{2,1,0:T(8,128)(2,1)} %stick_attention.1), calls=%async_computation.1 | async-start | bytes 524288 | tf_op jit(solution)/shard_map/all_to_all | solution.py:479
  (42 other events, 661.5 us)
where the time goes:
time: 221 us; the launch traced here: 220 us
  starting transfers between devices  83.6 us (38%)
  Pallas kernels  65 us (29%)
  waiting for transfers between devices  54.5 us (25%)
  local copies, waits for them, and re-layouts  8.36 us (4%)
  matrix products  7.47 us (3%)
    pallas_call x1, Pallas kernels, stick_attention(): pl.pallas_call(stick_kernel, out_shape=jax.ShapeDtypeStruct((16, 64, 128)...  34.6 us
    ppermute x12, waiting for transfers between devices, on_device(): around = lambda axis, v: [v] + [ring(axis, 4, d)(v) for d in (1, 2, 3)]  29 us
    ppermute x7, starting transfers between devices, on_device(): functools.partial(lax.ppermute, axis_name=Z, perm=[(i, i + d) for i in ra...  20 us
    ppermute x12, starting transfers between devices, on_device(): around = lambda axis, v: [v] + [ring(axis, 4, d)(v) for d in (1, 2, 3)]  18.5 us
    pallas_call x1, Pallas kernels, delta_local(): pl.pallas_call(delta_kernel, out_shape=(jax.ShapeDtypeStruct((1024, 128),...  17.8 us
    all_to_all x1, starting transfers between devices, on_device(): sb = lax.all_to_all(sb, (*Z, 'tp'), 0, 0, tiled=True)  12.2 us
    all_to_all x1, starting transfers between devices, on_device(): dm = lax.all_to_all(dm.reshape(8, 128, 128), ('y', 'tp'), 0, 0, tiled=True)  9.8 us
    ppermute x14, starting transfers between devices, on_device(): swap = lambda v: across(v)  9.69 us
  transfers between devices with their start and end apart: 43, of which 12 were waited for; matrix products, arithmetic and copies ran while one was open for 6% of the time, Pallas kernels for 30%

commit v1 on v0

--- a/solution.py
+++ b/solution.py
@@ -383,11 +383,11 @@
     )(place, scale, bias, decay_w, write_w, *shifts, *weights, *own, *other)
 
 
-def finish_kernel(gain_ref, qf_ref, of_ref, *refs):
-    maps, o_ref = refs[:-1], refs[-1]
+def finish_kernel(gain_ref, place, qf_ref, of_ref, maps, o_ref):
     state = jnp.zeros((128, 128), f32)
-    for ref in maps:
-        state = mm(ref[:, :128], state) + ref[:, 128:].astype(f32)
+    for n in range(7):
+        moved = mm(maps[n, :, :128], state) + maps[n, :, 128:].astype(f32)
+        state = jnp.where(n < place[3], moved, state)
     for t in range(4):
         rows = slice(t * CH, (t + 1) * CH)
         o = mm(qf_ref[rows, :], state) + of_ref[rows, :]
@@ -395,16 +395,16 @@
         o_ref[rows, :] = o.astype(bf16)
 
 
-def delta_finish(gain, qf, of, maps):
+def delta_finish(gain, place, qf, of, maps):
     vmem = pl.BlockSpec(memory_space=pltpu.VMEM)
     return pl.pallas_call(
         finish_kernel,
         out_shape=jax.ShapeDtypeStruct((1024, 128), bf16),
-        in_specs=[vmem] * (3 + len(maps)),
+        in_specs=[vmem, pl.BlockSpec(memory_space=pltpu.SMEM), vmem, vmem, vmem],
         out_specs=vmem,
         cost_estimate=pl.CostEstimate(flops=1_000_000_000, bytes_accessed=2_000_000, transcendentals=2_000),
         name="delta_finish",
-    )(gain, qf, of, *maps)
+    )(gain, place, qf, of, maps)
 
 
 def ring(axis, size, step):
@@ -455,7 +455,7 @@
     other_l = [swap(v) for v in (l1, l2, l3, l4)]
     shifts = around("y", decay_shift.reshape(4, 256))
 
-    place = jnp.stack([y, fs, tp]).astype(jnp.int32)
+    place = jnp.stack([y, fs, tp, z]).astype(jnp.int32)
     q, kv = stick_project(
         place,
         weights,
@@ -466,16 +466,14 @@
     qf, of, end = delta_local(
         place, decay_log_scale, write_bias, decay_w.T, write_w.T, weights, at_y, other_y, shifts
     )
-    ends = [
-        functools.partial(lax.ppermute, axis_name=Z, perm=[(i, i + d) for i in range(8 - d)])(end)
-        for d in range(7, 0, -1)
-    ]
-    dm = delta_finish(head_gain.reshape(1, 128), qf, of, ends)
+    ends = lax.all_to_all(jnp.broadcast_to(end[None], (8, 128, 256)), Z, 0, 0, tiled=True)
+    dm = delta_finish(head_gain.reshape(1, 128), place, qf, of, ends)
     dm = lax.all_to_all(dm.reshape(8, 128, 128), ("y", "tp"), 0, 0, tiled=True)
     outs_other = [swap(sb_out_w), swap(delta_out_w)]
 
     u = jnp.asarray(np.tril(np.ones((CH, CH), np.float32), -1), bf16)
-    sb = stick_attention(item(jnp.asarray(work_list()), 4 * z + y), sb_offset, q, u, kvs)
+    table = item(jnp.asarray(work_list()), 4 * z + y)
+    sb = stick_attention(table, sb_offset, q, u, kvs)
     sb = lax.all_to_all(sb, (*Z, "tp"), 0, 0, tiled=True)
 
     sb = sb.reshape(8, 2, 64, 2, 64).transpose(1, 3, 2, 0, 4).reshape(2, 128, 512)

time: 221 us -> 210 us (0.950)
  the two profiles are of different devices: /device:TPU:25 before, /device:TPU:31 now
where the time goes in v1:
time: 210 us; the launch traced here: 209 us
  waiting for transfers between devices  75.5 us (36%)
  Pallas kernels  65.1 us (31%)
  starting transfers between devices  48.2 us (23%)
  local copies, waits for them, and re-layouts  12.3 us (6%)
  matrix products  7.47 us (4%)
    ppermute x12, waiting for transfers between devices, on_device(): around = lambda axis, v: [v] + [ring(axis, 4, d)(v) for d in (1, 2, 3)]  47.5 us
    pallas_call x1, Pallas kernels, stick_attention(): pl.pallas_call(stick_kernel, out_shape=jax.ShapeDtypeStruct((16, 64, 128)...  34.6 us
    pallas_call x1, Pallas kernels, delta_local(): pl.pallas_call(delta_kernel, out_shape=(jax.ShapeDtypeStruct((1024, 128),...  17.8 us
    all_to_all x1, waiting for transfers between devices, on_device(): dm = lax.all_to_all(dm.reshape(8, 128, 128), ('y', 'tp'), 0, 0, tiled=True)  13.3 us
    pallas_call x1, Pallas kernels, stick_project(): pl.pallas_call(project_kernel, out_shape=(shape, shape), in_specs=[pl.Blo...  9.05 us
    all_to_all x1, waiting for transfers between devices, on_device(): sb = lax.all_to_all(sb, (*Z, 'tp'), 0, 0, tiled=True)  9.02 us
    ppermute x14, starting transfers between devices, on_device(): swap = lambda v: across(v)  8.64 us
    all_to_all x1, starting transfers between devices, on_device(): sb = lax.all_to_all(sb, (*Z, 'tp'), 0, 0, tiled=True)  8.16 us
  transfers between devices with their start and end apart: 37, of which 11 were waited for; matrix products, arithmetic and copies ran while one was open for 7% of the time, Pallas kernels for 31%

profile of v1, /device:TPU:31, one launch (start us, length us, event | category | flops | bytes accessed | tf_op | source)
XLA Modules:
  0.0 209.5 jit_solution(8179295705949818102)
XLA Ops:
  1.6 4.0 %collective-permute-start.15 = (bf16[256,1024]{1,0:T(8,128)(2,1)}, bf16[256,1024]{1,0:T(8,128)(2,1)S(1)}, u32[]{:S(2)}, u32[]{:S(2)}) collective-permute-start(bf16[256,1024]{1,0:T(8,128)(2,1)} %bitcast.42), channel_id=1, source_target_pairs={{0,224},{32,0},{64,32},{96,64},{128,96},{160,128},{192,160},{224,1... | collective-permute-start | bytes 1572872 | tf_op jit(solution)/shard_map/ppermute | solution.py:447
  10.0 10.5 %collective-permute-done.refs_1_ = f32[4,256]{1,0:T(4,128)S(1)} collective-permute-done((f32[4,256]{1,0:T(4,128)}, f32[4,256]{1,0:T(4,128)S(1)}, u32[]{:S(2)}, u32[]{:S(2)}) %collective-permute-start) | collective-permute-done | bytes 4128 | tf_op jit(solution)/shard_map/ppermute | solution.py:438
  22.5 2.2 %collective-permute-done.1.refs_2_ = f32[4,256]{1,0:T(4,128)S(1)} collective-permute-done((f32[4,256]{1,0:T(4,128)}, f32[4,256]{1,0:T(4,128)S(1)}, u32[]{:S(2)}, u32[]{:S(2)}) %collective-permute-start.1) | collective-permute-done | bytes 4128 | tf_op jit(solution)/shard_map/ppermute | solution.py:438
  30.1 2.7 %collective-permute-start.17 = (bf16[256,1024]{1,0:T(8,128)(2,1)S(1)}, bf16[256,1024]{1,0:T(8,128)(2,1)S(1)}, u32[]{:S(2)}, u32[]{:S(2)}) collective-permute-start(bf16[256,1024]{1,0:T(8,128)(2,1)S(1)} %collective-permute-done.15.refs_6_), channel_id=1, source_target_pairs={{0,224},{32,0},{64,32},{96,64},{128,96},{160,128},{192,160},{224,1... | collective-permute-start | bytes 1572872 | tf_op jit(solution)/shard_map/ppermute | solution.py:450
  32.8 7.8 %collective-permute-done.7.refs_10_ = bf16[256,1024]{1,0:T(8,128)(2,1)} collective-permute-done((bf16[256,1024]{1,0:T(8,128)(2,1)S(1)}, bf16[256,1024]{1,0:T(8,128)(2,1)}, u32[]{:S(2)}, u32[]{:S(2)}) %collective-permute-start.7) | collective-permute-done | bytes 524320 | tf_op jit(solution)/shard_map/ppermute | solution.py:438
  41.8 13.5 %collective-permute-done.8.refs_11_ = bf16[256,1024]{1,0:T(8,128)(2,1)} collective-permute-done((bf16[256,1024]{1,0:T(8,128)(2,1)S(1)}, bf16[256,1024]{1,0:T(8,128)(2,1)}, u32[]{:S(2)}, u32[]{:S(2)}) %collective-permute-start.8) | collective-permute-done | bytes 524320 | tf_op jit(solution)/shard_map/ppermute | solution.py:438
  56.6 2.9 %collective-permute-start.19 = (bf16[256,1024]{1,0:T(8,128)(2,1)S(1)}, bf16[256,1024]{1,0:T(8,128)(2,1)S(1)}, u32[]{:S(2)}, u32[]{:S(2)}) collective-permute-start(bf16[256,1024]{1,0:T(8,128)(2,1)S(1)} %collective-permute-done.17.refs_8_), channel_id=1, source_target_pairs={{0,224},{32,0},{64,32},{96,64},{128,96},{160,128},{192,160},{224,1... | collective-permute-start | bytes 1572872 | tf_op jit(solution)/shard_map/ppermute | solution.py:451
  59.5 2.5 %collective-permute-start.23 = (bf16[256,1024]{1,0:T(8,128)(2,1)}, bf16[256,1024]{1,0:T(8,128)(2,1)}, u32[]{:S(2)}, u32[]{:S(2)}) collective-permute-start(bf16[256,1024]{1,0:T(8,128)(2,1)} %copy-done.9), channel_id=1, source_target_pairs={{0,1},{1,0},{2,3},{3,2},{4,5},{5,4},{6,7},{7,6},{8,9},{9,8},{10,11... | collective-permute-start | bytes 1572872 | tf_op jit(solution)/shard_map/ppermute | solution.py:436
  62.1 11.9 %collective-permute-done.5.refs_7_.refs_3_ = bf16[512,640]{1,0:T(8,128)(2,1)S(1)} collective-permute-done((bf16[512,640]{1,0:T(8,128)(2,1)S(1)}, bf16[512,640]{1,0:T(8,128)(2,1)S(1)}, u32[]{:S(2)}, u32[]{:S(2)}) %collective-permute-start.5) | collective-permute-done | bytes 655392 | tf_op jit(solution)/shard_map/ppermute | solution.py:438
  78.3 2.7 %collective-permute-start.21 = (bf16[128,1024]{1,0:T(8,128)(2,1)}, bf16[128,1024]{1,0:T(8,128)(2,1)}, u32[]{:S(2)}, u32[]{:S(2)}) collective-permute-start(bf16[128,1024]{1,0:T(8,128)(2,1)} %slice.9), channel_id=1, source_target_pairs={{0,224},{32,0},{64,32},{96,64},{128,96},{160,128},{192,160},{224,1... | collective-permute-start | bytes 786440 | tf_op jit(solution)/shard_map/ppermute | solution.py:452
  81.9 17.8 %delta_local.1 = (f32[1024,128]{1,0:T(8,128)}, f32[1024,128]{1,0:T(8,128)}, bf16[128,256]{1,0:T(8,128)(2,1)}) custom-call(s32[4]{0:T(128)} %pad_add_fusion.place, f32[4]{0:T(128)} %scale_ref.1, f32[4]{0:T(128)} %bias_ref.1, bf16[4,2048]{1,0:T(4,128)(2,1)} %bitcast.50, bf16[4,2048]{1,0:T(4,128)(2,1)} %bitcast.51, f32[4,256]{1,0:T(4,128)} %bitcast.55, ...), custom_call_target="tpu_custom_call" | custom-call | flops 12000000000 | bytes 8000000 | tf_op jit(solution)/shard_map/delta_local/pallas_call | solution.py:361
  99.8 1.7 broadcast_in_dim.10
  101.5 5.5 %all-to-all-start = ((bf16[8,128,256]{2,1,0:T(8,128)(2,1)}), bf16[8,128,256]{2,1,0:T(8,128)(2,1)S(1)}, u32[]{:S(2)}, u32[]{:S(2)}) async-start(bf16[8,128,256]{2,1,0:T(8,128)(2,1)} %broadcast_in_dim.10), calls=%async_computation | async-start | bytes 1048576 | tf_op jit(solution)/shard_map/all_to_all | solution.py:469
  110.2 9.0 %stick_project.1 = (bf16[8,256,128]{2,1,0:T(8,128)(2,1)}, bf16[8,256,128]{2,1,0:T(8,128)(2,1)}) custom-call(s32[4]{0:T(128)} %pad_add_fusion.place, bf16[512,640]{1,0:T(8,128)(2,1)} %copy-done.1, bf16[512,640]{1,0:T(8,128)(2,1)} %copy-done.5, bf16[512,640]{1,0:T(8,128)(2,1)} %copy-done.6, bf16[512,640]{1,0:T(8,128)(2,1)} %copy-done.7, ...), custom_call_target="tpu_custom_call" | custom-call | flops 2200000000 | bytes 10000000 | tf_op jit(solution)/shard_map/stick_project/pallas_call | solution.py:218
  120.8 4.1 %all-to-all-done.maps = bf16[8,128,256]{2,1,0:T(8,128)(2,1)S(1)} async-done(((bf16[8,128,256]{2,1,0:T(8,128)(2,1)}), bf16[8,128,256]{2,1,0:T(8,128)(2,1)S(1)}, u32[]{:S(2)}, u32[]{:S(2)}) %all-to-all-start) | async-done | bytes 524320 | tf_op jit(solution)/shard_map/all_to_all | solution.py:469
  125.7 3.5 %delta_finish.1 = bf16[1024,128]{1,0:T(8,128)(2,1)} custom-call(f32[1,128]{1,0:T(1,128)} %bitcast.56, s32[4]{0:T(128)} %pad_add_fusion.place, f32[1024,128]{1,0:T(8,128)} %get-tuple-element.10.qf_ref, f32[1024,128]{1,0:T(8,128)} %get-tuple-element.11.of_ref, bf16[8,128,256]{2,1,0:T(8,128)(2,1)} %copy-done.13), custom_call_target="tpu_custom_call" | custom-call | flops 1000000000 | bytes 2000000 | tf_op jit(solution)/shard_map/delta_finish/pallas_call | solution.py:400
  129.2 4.6 %all-to-all-start.1 = ((bf16[8,128,128]{2,1,0:T(8,128)(2,1)}), bf16[8,128,128]{2,1,0:T(8,128)(2,1)S(1)}, u32[]{:S(2)}, u32[]{:S(2)}) async-start(bf16[8,128,128]{2,1,0:T(8,128)(2,1)} %bitcast.49), calls=%async_computation.1 | async-start | bytes 524288 | tf_op jit(solution)/shard_map/all_to_all | solution.py:471
  135.6 13.3 %all-to-all-done.1 = bf16[8,128,128]{2,1,0:T(8,128)(2,1)S(1)} async-done(((bf16[8,128,128]{2,1,0:T(8,128)(2,1)}), bf16[8,128,128]{2,1,0:T(8,128)(2,1)S(1)}, u32[]{:S(2)}, u32[]{:S(2)}) %all-to-all-start.1) | async-done | bytes 262176 | tf_op jit(solution)/shard_map/all_to_all | solution.py:471
  149.2 34.6 %stick_attention.1 = bf16[16,64,128]{2,1,0:T(8,128)(2,1)} custom-call(s32[384]{0:T(512)} %fusion.17.table, f32[8]{0:T(128)} %off_ref.1, bf16[8,256,128]{2,1,0:T(8,128)(2,1)} %get-tuple-element.13.q, bf16[256,256]{1,0:T(8,128)(2,1)} %constant.55.clone.u_ref, bf16[8,256,128]{2,1,0:T(8,128)(2,1)} %get-tuple-element.14.refs_0_, ...), custom_call_target="tpu_custom_call" | custom-call | flops 20000000000 | bytes 4000000 | tf_op jit(solution)/shard_map/stick_attention/pallas_call | solution.py:139
  183.8 8.2 %all-to-all-start.2 = ((bf16[16,64,128]{2,1,0:T(8,128)(2,1)}), bf16[16,64,128]{2,1,0:T(8,128)(2,1)S(1)}, u32[]{:S(2)}, u32[]{:S(2)}) async-start(bf16[16,64,128]{2,1,0:T(8,128)(2,1)} %stick_attention.1), calls=%async_computation.2 | async-start | bytes 524288 | tf_op jit(solution)/shard_map/all_to_all | solution.py:477
  192.5 2.1 convolution_add_fusion.1
  194.6 9.0 %all-to-all-done.2 = bf16[16,64,128]{2,1,0:T(8,128)(2,1)S(1)} async-done(((bf16[16,64,128]{2,1,0:T(8,128)(2,1)}), bf16[16,64,128]{2,1,0:T(8,128)(2,1)S(1)}, u32[]{:S(2)}, u32[]{:S(2)}) %all-to-all-start.2) | async-done | bytes 262176 | tf_op jit(solution)/shard_map/all_to_all | solution.py:477
  204.5 2.0 fusion.4
  206.6 2.9 %fusion.2 = bf16[1,128,2048]{2,1,0:T(8,128)(2,1)} fusion(f32[128,2048]{1,0:T(8,128)S(1)} %convolution_add_fusion.1, f32[128,2048]{1,0:T(8,128)S(1)} %fusion.4, bf16[512,2048]{1,0:T(8,128)(2,1)} %collective-permute-done.33, bf16[2,128,512]{2,1,0:T(8,128)(2,1)S(1)} %reshape.35, s32[]{:T(128)S(6)} %select_n.26), kind=kOutput, calls=%fused_computation.4 | convolution fusion | flops 269221888 | bytes 4849668 | tf_op jit(solution)/shard_map/dot_general | solution.py:483
  (111 shorter events, 30.0 us)
Async XLA Ops:
  0.0 29.1 %collective-permute-start.14 = (bf16[256,1024]{1,0:T(8,128)(2,1)}, bf16[256,1024]{1,0:T(8,128)(2,1)}, u32[]{:S(2)}, u32[]{:S(2)}) collective-permute-start(bf16[256,1024]{1,0:T(8,128)(2,1)} %bitcast.41), channel_id=1, source_target_pairs={{0,32},{32,64},{64,96},{96,128},{128,160},{160,192},{192,224},{224... | collective-permute-start | bytes 1572872 | tf_op jit(solution)/shard_map/ppermute | solution.py:447
  1.6 28.3 %collective-permute-start.15 = (bf16[256,1024]{1,0:T(8,128)(2,1)}, bf16[256,1024]{1,0:T(8,128)(2,1)S(1)}, u32[]{:S(2)}, u32[]{:S(2)}) collective-permute-start(bf16[256,1024]{1,0:T(8,128)(2,1)} %bitcast.42), channel_id=1, source_target_pairs={{0,224},{32,0},{64,32},{96,64},{128,96},{160,128},{192,160},{224,1... | collective-permute-start | bytes 1572872 | tf_op jit(solution)/shard_map/ppermute | solution.py:447
  5.7 24.5 %collective-permute-start.9 = (bf16[256,1024]{1,0:T(8,128)(2,1)}, bf16[256,1024]{1,0:T(8,128)(2,1)S(1)}, u32[]{:S(2)}, u32[]{:S(2)}) collective-permute-start(bf16[256,1024]{1,0:T(8,128)(2,1)} %bitcast.43), channel_id=1, source_target_pairs={{0,1},{1,0},{2,3},{3,2},{4,5},{5,4},{6,7},{7,6},{8,9},{9,8},{10,11... | collective-permute-start | bytes 1572872 | tf_op jit(solution)/shard_map/ppermute | solution.py:436
  6.6 23.5 %collective-permute-start.6 = (bf16[256,1024]{1,0:T(8,128)(2,1)}, bf16[256,1024]{1,0:T(8,128)(2,1)}, u32[]{:S(2)}, u32[]{:S(2)}) collective-permute-start(bf16[256,1024]{1,0:T(8,128)(2,1)} %bitcast.44), channel_id=1, source_target_pairs={{0,8},{8,16},{16,24},{24,0},{1,9},{9,17},{17,25},{25,1},{2,10},{10... | collective-permute-start | bytes 1572872 | tf_op jit(solution)/shard_map/ppermute | solution.py:438
  29.1 26.1 %collective-permute-start.8 = (bf16[256,1024]{1,0:T(8,128)(2,1)S(1)}, bf16[256,1024]{1,0:T(8,128)(2,1)}, u32[]{:S(2)}, u32[]{:S(2)}) collective-permute-start(bf16[256,1024]{1,0:T(8,128)(2,1)S(1)} %bitcast.48), channel_id=1, source_target_pairs={{0,24},{8,0},{16,8},{24,16},{1,25},{9,1},{17,9},{25,17},{2,26},{10... | collective-permute-start | bytes 1572872 | tf_op jit(solution)/shard_map/ppermute | solution.py:438
  29.9 25.9 %collective-permute-start.3 = (bf16[512,640]{1,0:T(8,128)(2,1)S(1)}, bf16[512,640]{1,0:T(8,128)(2,1)S(1)}, u32[]{:S(2)}, u32[]{:S(2)}) collective-permute-start(bf16[512,640]{1,0:T(8,128)(2,1)S(1)} %concatenate.3.refs_4_.refs_0_), channel_id=1, source_target_pairs={{0,2},{2,4},{4,6},{6,0},{1,3},{3,5},{5,7},{7,1},{8,10},{10,12},{12... | collective-permute-start | bytes 1966088 | tf_op jit(solution)/shard_map/ppermute | solution.py:438
  30.1 26.5 %collective-permute-start.16 = (bf16[256,1024]{1,0:T(8,128)(2,1)}, bf16[256,1024]{1,0:T(8,128)(2,1)}, u32[]{:S(2)}, u32[]{:S(2)}) collective-permute-start(bf16[256,1024]{1,0:T(8,128)(2,1)} %collective-permute-done.14.refs_5_), channel_id=1, source_target_pairs={{0,32},{32,64},{64,96},{96,128},{128,160},{160,192},{192,224},{224... | collective-permute-start | bytes 1572872 | tf_op jit(solution)/shard_map/ppermute | solution.py:450
  30.1 26.5 %collective-permute-start.17 = (bf16[256,1024]{1,0:T(8,128)(2,1)S(1)}, bf16[256,1024]{1,0:T(8,128)(2,1)S(1)}, u32[]{:S(2)}, u32[]{:S(2)}) collective-permute-start(bf16[256,1024]{1,0:T(8,128)(2,1)S(1)} %collective-permute-done.15.refs_6_), channel_id=1, source_target_pairs={{0,224},{32,0},{64,32},{96,64},{128,96},{160,128},{192,160},{224,1... | collective-permute-start | bytes 1572872 | tf_op jit(solution)/shard_map/ppermute | solution.py:450
  40.6 18.9 %collective-permute-start.4 = (bf16[512,640]{1,0:T(8,128)(2,1)S(1)}, bf16[512,640]{1,0:T(8,128)(2,1)S(1)}, u32[]{:S(2)}, u32[]{:S(2)}) collective-permute-start(bf16[512,640]{1,0:T(8,128)(2,1)S(1)} %concatenate.3.refs_4_.refs_0_), channel_id=1, source_target_pairs={{0,4},{2,6},{4,0},{6,2},{1,5},{3,7},{5,1},{7,3},{8,12},{10,14},{12... | collective-permute-start | bytes 1966088 | tf_op jit(solution)/shard_map/ppermute | solution.py:438
  55.8 19.1 %collective-permute-start.22 = (bf16[256,1024]{1,0:T(8,128)(2,1)}, bf16[256,1024]{1,0:T(8,128)(2,1)S(1)}, u32[]{:S(2)}, u32[]{:S(2)}) collective-permute-start(bf16[256,1024]{1,0:T(8,128)(2,1)} %collective-permute-done.14.refs_5_), channel_id=1, source_target_pairs={{0,1},{1,0},{2,3},{3,2},{4,5},{5,4},{6,7},{7,6},{8,9},{9,8},{10,11... | collective-permute-start | bytes 1572872 | tf_op jit(solution)/shard_map/ppermute | solution.py:436
  56.6 18.8 %collective-permute-start.19 = (bf16[256,1024]{1,0:T(8,128)(2,1)S(1)}, bf16[256,1024]{1,0:T(8,128)(2,1)S(1)}, u32[]{:S(2)}, u32[]{:S(2)}) collective-permute-start(bf16[256,1024]{1,0:T(8,128)(2,1)S(1)} %collective-permute-done.17.refs_8_), channel_id=1, source_target_pairs={{0,224},{32,0},{64,32},{96,64},{128,96},{160,128},{192,160},{224,1... | collective-permute-start | bytes 1572872 | tf_op jit(solution)/shard_map/ppermute | solution.py:451
  78.0 30.0 %collective-permute-start.25 = (bf16[256,1024]{1,0:T(8,128)(2,1)}, bf16[256,1024]{1,0:T(8,128)(2,1)}, u32[]{:S(2)}, u32[]{:S(2)}) collective-permute-start(bf16[256,1024]{1,0:T(8,128)(2,1)} %copy-done.11), channel_id=1, source_target_pairs={{0,1},{1,0},{2,3},{3,2},{4,5},{5,4},{6,7},{7,6},{8,9},{9,8},{10,11... | collective-permute-start | bytes 1572872 | tf_op jit(solution)/shard_map/ppermute | solution.py:436
  78.3 28.6 %collective-permute-start.20 = (bf16[128,1024]{1,0:T(8,128)(2,1)}, bf16[128,1024]{1,0:T(8,128)(2,1)}, u32[]{:S(2)}, u32[]{:S(2)}) collective-permute-start(bf16[128,1024]{1,0:T(8,128)(2,1)} %slice.8), channel_id=1, source_target_pairs={{0,32},{32,64},{64,96},{96,128},{128,160},{160,192},{192,224},{224... | collective-permute-start | bytes 786440 | tf_op jit(solution)/shard_map/ppermute | solution.py:452
  78.3 29.4 %collective-permute-start.21 = (bf16[128,1024]{1,0:T(8,128)(2,1)}, bf16[128,1024]{1,0:T(8,128)(2,1)}, u32[]{:S(2)}, u32[]{:S(2)}) collective-permute-start(bf16[128,1024]{1,0:T(8,128)(2,1)} %slice.9), channel_id=1, source_target_pairs={{0,224},{32,0},{64,32},{96,64},{128,96},{160,128},{192,160},{224,1... | collective-permute-start | bytes 786440 | tf_op jit(solution)/shard_map/ppermute | solution.py:452
  81.0 28.4 %collective-permute-start.26 = (bf16[256,1024]{1,0:T(8,128)(2,1)S(1)}, bf16[256,1024]{1,0:T(8,128)(2,1)}, u32[]{:S(2)}, u32[]{:S(2)}) collective-permute-start(bf16[256,1024]{1,0:T(8,128)(2,1)S(1)} %collective-permute-done.18.refs_9_), channel_id=1, source_target_pairs={{0,1},{1,0},{2,3},{3,2},{4,5},{5,4},{6,7},{7,6},{8,9},{9,8},{10,11... | collective-permute-start | bytes 1572872 | tf_op jit(solution)/shard_map/ppermute | solution.py:436
  81.8 27.7 %collective-permute-start.27 = (bf16[256,1024]{1,0:T(8,128)(2,1)S(1)}, bf16[256,1024]{1,0:T(8,128)(2,1)}, u32[]{:S(2)}, u32[]{:S(2)}) collective-permute-start(bf16[256,1024]{1,0:T(8,128)(2,1)S(1)} %collective-permute-done.19.refs_10_), channel_id=1, source_target_pairs={{0,1},{1,0},{2,3},{3,2},{4,5},{5,4},{6,7},{7,6},{8,9},{9,8},{10,11... | collective-permute-start | bytes 1572872 | tf_op jit(solution)/shard_map/ppermute | solution.py:436
  101.5 23.4 %all-to-all-start = ((bf16[8,128,256]{2,1,0:T(8,128)(2,1)}), bf16[8,128,256]{2,1,0:T(8,128)(2,1)S(1)}, u32[]{:S(2)}, u32[]{:S(2)}) async-start(bf16[8,128,256]{2,1,0:T(8,128)(2,1)} %broadcast_in_dim.10), calls=%async_computation | async-start | bytes 1048576 | tf_op jit(solution)/shard_map/all_to_all | solution.py:469
  119.2 29.9 %collective-permute-start.30 = (bf16[8,256,128]{2,1,0:T(8,128)(2,1)}, bf16[8,256,128]{2,1,0:T(8,128)(2,1)}, u32[]{:S(2)}, u32[]{:S(2)}) collective-permute-start(bf16[8,256,128]{2,1,0:T(8,128)(2,1)} %get-tuple-element.14.refs_0_), channel_id=1, source_target_pairs={{0,8},{8,16},{16,24},{24,0},{1,9},{9,17},{17,25},{25,1},{2,10},{10... | collective-permute-start | bytes 1572872 | tf_op jit(solution)/shard_map/ppermute | solution.py:438
  119.9 29.3 %collective-permute-start.31 = (bf16[8,256,128]{2,1,0:T(8,128)(2,1)}, bf16[8,256,128]{2,1,0:T(8,128)(2,1)}, u32[]{:S(2)}, u32[]{:S(2)}) collective-permute-start(bf16[8,256,128]{2,1,0:T(8,128)(2,1)} %get-tuple-element.14.refs_0_), channel_id=1, source_target_pairs={{0,16},{8,24},{16,0},{24,8},{1,17},{9,25},{17,1},{25,9},{2,18},{10... | collective-permute-start | bytes 1572872 | tf_op jit(solution)/shard_map/ppermute | solution.py:438
  119.9 29.3 %collective-permute-start.32 = (bf16[8,256,128]{2,1,0:T(8,128)(2,1)}, bf16[8,256,128]{2,1,0:T(8,128)(2,1)}, u32[]{:S(2)}, u32[]{:S(2)}) collective-permute-start(bf16[8,256,128]{2,1,0:T(8,128)(2,1)} %get-tuple-element.14.refs_0_), channel_id=1, source_target_pairs={{0,24},{8,0},{16,8},{24,16},{1,25},{9,1},{17,9},{25,17},{2,26},{10... | collective-permute-start | bytes 1572872 | tf_op jit(solution)/shard_map/ppermute | solution.py:438
  129.2 19.8 %all-to-all-start.1 = ((bf16[8,128,128]{2,1,0:T(8,128)(2,1)}), bf16[8,128,128]{2,1,0:T(8,128)(2,1)S(1)}, u32[]{:S(2)}, u32[]{:S(2)}) async-start(bf16[8,128,128]{2,1,0:T(8,128)(2,1)} %bitcast.49), calls=%async_computation.1 | async-start | bytes 524288 | tf_op jit(solution)/shard_map/all_to_all | solution.py:471
  133.8 58.6 %collective-permute-start.13 = (bf16[512,2048]{1,0:T(8,128)(2,1)S(1)}, bf16[512,2048]{1,0:T(8,128)(2,1)}, u32[]{:S(2)}, u32[]{:S(2)}) collective-permute-start(bf16[512,2048]{1,0:T(8,128)(2,1)S(1)} %copy-done.2), channel_id=1, source_target_pairs={{0,1},{1,0},{2,3},{3,2},{4,5},{5,4},{6,7},{7,6},{8,9},{9,8},{10,11... | collective-permute-start | bytes 6291464 | tf_op jit(solution)/shard_map/ppermute | solution.py:436
  134.2 72.3 %collective-permute-start.33 = (bf16[512,2048]{1,0:T(8,128)(2,1)}, bf16[512,2048]{1,0:T(8,128)(2,1)}, u32[]{:S(2)}, u32[]{:S(2)}) collective-permute-start(bf16[512,2048]{1,0:T(8,128)(2,1)} %param.32), channel_id=1, source_target_pairs={{0,1},{1,0},{2,3},{3,2},{4,5},{5,4},{6,7},{7,6},{8,9},{9,8},{10,11... | collective-permute-start | bytes 6291464 | tf_op jit(solution)/shard_map/ppermute | solution.py:436
  183.8 19.7 %all-to-all-start.2 = ((bf16[16,64,128]{2,1,0:T(8,128)(2,1)}), bf16[16,64,128]{2,1,0:T(8,128)(2,1)S(1)}, u32[]{:S(2)}, u32[]{:S(2)}) async-start(bf16[16,64,128]{2,1,0:T(8,128)(2,1)} %stick_attention.1), calls=%async_computation.2 | async-start | bytes 524288 | tf_op jit(solution)/shard_map/all_to_all | solution.py:477
  (32 other events, 552.0 us)

commit v2 on v0

--- a/solution.py
+++ b/solution.py
@@ -86,45 +86,53 @@
 
     lax.fori_loop(0, 4, diagonal, 0)
 
-    def one(n, carry):
-        for k in range(2):
-            tile((table[SINGLE + 16 * k + n],), table[SINGLE + 16 * k + 8 + n], False)
-        return carry
-
-    lax.fori_loop(0, 8, one, 0)
-
-    def step(n):
-        return (table[PAIRS + n], table[PAIRS + 64 + n]), table[PAIRS + 128 + n]
-
-    def scores(n, late, sp_at):
-        slots, c = step(n)
-        z = jnp.dot(jnp.concatenate([q[s] for s in slots]), kt[c], preferred_element_type=f32) * (0.125 * LOG2E) + off
+    def pair_step(n):
+        c = table[PAIRS + 128 + n]
+        return (table[PAIRS + n], table[PAIRS + 64 + n]), (c,)
+
+    def single_step(n):
+        n = lax.rem(n, 8)
+        at = (SINGLE + n, SINGLE + 16 + n)
+        return tuple(table[k] for k in at), tuple(table[k + 8] for k in at)
+
+    def product(rows, columns, keys):
+        if len(keys) == 1:
+            return jnp.dot(jnp.concatenate(rows), columns[keys[0]], preferred_element_type=f32)
+        return jnp.concatenate([jnp.dot(r, columns[c], preferred_element_type=f32) for r, c in zip(rows, keys)])
+
+    def scores(step, late, sp_at):
+        slots, keys = step
+        z = product([q[s] for s in slots], kt, keys) * (0.125 * LOG2E) + off
         sp = jnp.maximum(jnp.log2(1.0 + jnp.exp2(jnp.minimum(z, 40.0))), z)
         late[...] = z - sp
         sp_at[...] = sp.astype(bf16)
 
-    def weigh(n, late, sp_at):
-        slots, c = step(n)
+    def weigh(step, late, sp_at):
+        slots, keys = step
         after = jnp.dot(sp_at[...], u_ref[...], preferred_element_type=f32)
         r = jnp.concatenate([run[s] for s in slots])
-        w = jnp.exp2(late[...] - (after + jnp.concatenate([r, r], axis=1)))
-        out = jnp.dot(w.astype(bf16), kvs[c], preferred_element_type=f32)
+        w = jnp.exp2(late[...] - (after + jnp.concatenate([r, r], axis=1))).astype(bf16)
+        out = product([w[:CH], w[CH:]], kvs, keys)
         total = r + (after[:, :1] + sp_at[:, :1].astype(f32))
         for k, s in enumerate(slots):
             rows = slice(k * CH, k * CH + CH)
             run[s] = total[rows]
             acc[s] += out[rows]
 
-    scores(0, late_a, sp_a)
-
-    def two(m, carry):
-        weigh(2 * m, late_a, sp_a)
-        scores(2 * m + 1, late_b, sp_b)
-        weigh(2 * m + 1, late_b, sp_b)
-        scores(2 * m + 2, late_a, sp_a)
-        return carry
-
-    lax.fori_loop(0, table[COUNT] // 2, two, 0)
+    def sweep(step, pairs_of_steps):
+        scores(step(0), late_a, sp_a)
+
+        def two(m, carry):
+            weigh(step(2 * m), late_a, sp_a)
+            scores(step(2 * m + 1), late_b, sp_b)
+            weigh(step(2 * m + 1), late_b, sp_b)
+            scores(step(2 * m + 2), late_a, sp_a)
+            return carry
+
+        lax.fori_loop(0, pairs_of_steps, two, 0)
+
+    sweep(single_step, 4)
+    sweep(pair_step, table[COUNT] // 2)
     lane = lax.broadcasted_iota(jnp.int32, (64, 128), 1)
     for i in range(8):
         rows = acc[table[SLOTS + i]]
@@ -475,7 +483,8 @@
     outs_other = [swap(sb_out_w), swap(delta_out_w)]
 
     u = jnp.asarray(np.tril(np.ones((CH, CH), np.float32), -1), bf16)
-    sb = stick_attention(item(jnp.asarray(work_list()), 4 * z + y), sb_offset, q, u, kvs)
+    table = item(jnp.asarray(work_list()), 4 * z + y)
+    sb = stick_attention(table, sb_offset, q, u, kvs)
     sb = lax.all_to_all(sb, (*Z, "tp"), 0, 0, tiled=True)
 
     sb = sb.reshape(8, 2, 64, 2, 64).transpose(1, 3, 2, 0, 4).reshape(2, 128, 512)

time: 221 us -> 219 us (level)
  transfers between devices with their start and end apart: 43 -> 43, of which waited for: 12 -> 12; matrix products, arithmetic and copies ran while one was open for 6% -> 6% of each run, Pallas kernels for 30% -> 29%
where the time goes in v2:
time: 219 us
  starting transfers between devices  83.6 us (38%)
  Pallas kernels  63.7 us (29%)
  waiting for transfers between devices  54.5 us (25%)
  local copies, waits for them, and re-layouts  8.36 us (4%)
  matrix products  7.47 us (3%)
    pallas_call x1, Pallas kernels, stick_attention(): pl.pallas_call(stick_kernel, out_shape=jax.ShapeDtypeStruct((16, 64, 128)...  33.4 us
    ppermute x12, waiting for transfers between devices, on_device(): around = lambda axis, v: [v] + [ring(axis, 4, d)(v) for d in (1, 2, 3)]  29 us
    ppermute x7, starting transfers between devices, on_device(): functools.partial(lax.ppermute, axis_name=Z, perm=[(i, i + d) for i in ra...  20 us
    ppermute x12, starting transfers between devices, on_device(): around = lambda axis, v: [v] + [ring(axis, 4, d)(v) for d in (1, 2, 3)]  18.5 us
    pallas_call x1, Pallas kernels, delta_local(): pl.pallas_call(delta_kernel, out_shape=(jax.ShapeDtypeStruct((1024, 128),...  17.8 us
    all_to_all x1, starting transfers between devices, on_device(): sb = lax.all_to_all(sb, (*Z, 'tp'), 0, 0, tiled=True)  12.1 us
    all_to_all x1, starting transfers between devices, on_device(): dm = lax.all_to_all(dm.reshape(8, 128, 128), ('y', 'tp'), 0, 0, tiled=True)  9.8 us
    ppermute x14, starting transfers between devices, on_device(): swap = lambda v: across(v)  9.69 us
  transfers between devices with their start and end apart: 43, of which 12 were waited for; matrix products, arithmetic and copies ran while one was open for 6% of the time, Pallas kernels for 29%

profile of v2, /device:TPU:25, one launch (start us, length us, event | category | flops | bytes accessed | tf_op | source)
XLA Modules:
  0.0 218.7 jit_solution(5481515098494712595)
XLA Ops:
  1.6 4.0 %collective-permute-start.22 = (bf16[256,1024]{1,0:T(8,128)(2,1)}, bf16[256,1024]{1,0:T(8,128)(2,1)S(1)}, u32[]{:S(2)}, u32[]{:S(2)}) collective-permute-start(bf16[256,1024]{1,0:T(8,128)(2,1)} %bitcast.41), channel_id=1, source_target_pairs={{0,224},{32,0},{64,32},{96,64},{128,96},{160,128},{192,160},{224,1... | collective-permute-start | bytes 1572872 | tf_op jit(solution)/shard_map/ppermute | solution.py:455
  12.7 2.6 %collective-permute-done.2.refs_3_ = f32[4,256]{1,0:T(4,128)S(1)} collective-permute-done((f32[4,256]{1,0:T(4,128)}, f32[4,256]{1,0:T(4,128)S(1)}, u32[]{:S(2)}, u32[]{:S(2)}) %collective-permute-start.2) | collective-permute-done | bytes 4128 | tf_op jit(solution)/shard_map/ppermute | solution.py:446
  24.6 4.2 %collective-permute-done.7.refs_10_ = bf16[256,1024]{1,0:T(8,128)(2,1)} collective-permute-done((bf16[256,1024]{1,0:T(8,128)(2,1)}, bf16[256,1024]{1,0:T(8,128)(2,1)}, u32[]{:S(2)}, u32[]{:S(2)}) %collective-permute-start.7) | collective-permute-done | bytes 524320 | tf_op jit(solution)/shard_map/ppermute | solution.py:446
  28.8 2.7 %collective-permute-start.4 = (bf16[512,640]{1,0:T(8,128)(2,1)S(1)}, bf16[512,640]{1,0:T(8,128)(2,1)S(1)}, u32[]{:S(2)}, u32[]{:S(2)}) collective-permute-start(bf16[512,640]{1,0:T(8,128)(2,1)S(1)} %concatenate.3.refs_4_.refs_0_), channel_id=1, source_target_pairs={{0,4},{2,6},{4,0},{6,2},{1,5},{3,7},{5,1},{7,3},{8,12},{10,14},{12... | collective-permute-start | bytes 1966088 | tf_op jit(solution)/shard_map/ppermute | solution.py:446
  31.6 10.7 %collective-permute-done.8.refs_11_ = bf16[256,1024]{1,0:T(8,128)(2,1)} collective-permute-done((bf16[256,1024]{1,0:T(8,128)(2,1)}, bf16[256,1024]{1,0:T(8,128)(2,1)}, u32[]{:S(2)}, u32[]{:S(2)}) %collective-permute-start.8) | collective-permute-done | bytes 524320 | tf_op jit(solution)/shard_map/ppermute | solution.py:446
  45.5 2.9 %collective-permute-start.26 = (bf16[256,1024]{1,0:T(8,128)(2,1)S(1)}, bf16[256,1024]{1,0:T(8,128)(2,1)S(1)}, u32[]{:S(2)}, u32[]{:S(2)}) collective-permute-start(bf16[256,1024]{1,0:T(8,128)(2,1)S(1)} %collective-permute-done.24.refs_8_), channel_id=1, source_target_pairs={{0,224},{32,0},{64,32},{96,64},{128,96},{160,128},{192,160},{224,1... | collective-permute-start | bytes 1572872 | tf_op jit(solution)/shard_map/ppermute | solution.py:459
  48.4 3.2 %collective-permute-done.4.refs_6_.refs_2_ = bf16[512,640]{1,0:T(8,128)(2,1)S(1)} collective-permute-done((bf16[512,640]{1,0:T(8,128)(2,1)S(1)}, bf16[512,640]{1,0:T(8,128)(2,1)S(1)}, u32[]{:S(2)}, u32[]{:S(2)}) %collective-permute-start.4) | collective-permute-done | bytes 655392 | tf_op jit(solution)/shard_map/ppermute | solution.py:446
  54.1 7.6 %collective-permute-done.5.refs_7_.refs_3_ = bf16[512,640]{1,0:T(8,128)(2,1)S(1)} collective-permute-done((bf16[512,640]{1,0:T(8,128)(2,1)S(1)}, bf16[512,640]{1,0:T(8,128)(2,1)S(1)}, u32[]{:S(2)}, u32[]{:S(2)}) %collective-permute-start.5) | collective-permute-done | bytes 655392 | tf_op jit(solution)/shard_map/ppermute | solution.py:446
  65.6 2.7 %collective-permute-start.28 = (bf16[128,1024]{1,0:T(8,128)(2,1)}, bf16[128,1024]{1,0:T(8,128)(2,1)}, u32[]{:S(2)}, u32[]{:S(2)}) collective-permute-start(bf16[128,1024]{1,0:T(8,128)(2,1)} %slice.9), channel_id=1, source_target_pairs={{0,224},{32,0},{64,32},{96,64},{128,96},{160,128},{192,160},{224,1... | collective-permute-start | bytes 786440 | tf_op jit(solution)/shard_map/ppermute | solution.py:460
  70.2 4.4 %collective-permute-done.27.refs_11_ = bf16[128,1024]{1,0:T(8,128)(2,1)} collective-permute-done((bf16[128,1024]{1,0:T(8,128)(2,1)}, bf16[128,1024]{1,0:T(8,128)(2,1)}, u32[]{:S(2)}, u32[]{:S(2)}) %collective-permute-start.27) | collective-permute-done | bytes 262176 | tf_op jit(solution)/shard_map/ppermute | solution.py:460
  75.8 17.8 %delta_local.1 = (f32[1024,128]{1,0:T(8,128)}, f32[1024,128]{1,0:T(8,128)}, bf16[128,256]{1,0:T(8,128)(2,1)}) custom-call(s32[3]{0:T(128)} %pad_add_fusion.place, f32[4]{0:T(128)} %scale_ref.1, f32[4]{0:T(128)} %bias_ref.1, bf16[4,2048]{1,0:T(4,128)(2,1)} %bitcast.49, bf16[4,2048]{1,0:T(4,128)(2,1)} %bitcast.50, f32[4,256]{1,0:T(4,128)} %bitcast.54, ...), custom_call_target="tpu_custom_call" | custom-call | flops 12000000000 | bytes 8000000 | tf_op jit(solution)/shard_map/delta_local/pallas_call | solution.py:369
  93.7 4.7 %collective-permute-start.13 = (bf16[128,256]{1,0:T(8,128)(2,1)}, bf16[128,256]{1,0:T(8,128)(2,1)S(1)}, u32[]{:S(2)}, u32[]{:S(2)}) collective-permute-start(bf16[128,256]{1,0:T(8,128)(2,1)} %get-tuple-element.12), channel_id=1, source_target_pairs={{0,224},{1,225},{2,226},{3,227},{4,228},{5,229},{6,230},{7,231},{8... | collective-permute-start | bytes 196616 | tf_op jit(solution)/shard_map/ppermute | solution.py:478
  98.5 9.1 %stick_project.1 = (bf16[8,256,128]{2,1,0:T(8,128)(2,1)}, bf16[8,256,128]{2,1,0:T(8,128)(2,1)}) custom-call(s32[3]{0:T(128)} %pad_add_fusion.place, bf16[512,640]{1,0:T(8,128)(2,1)} %copy-done.1, bf16[512,640]{1,0:T(8,128)(2,1)} %copy-done.5, bf16[512,640]{1,0:T(8,128)(2,1)} %copy-done.6, bf16[512,640]{1,0:T(8,128)(2,1)} %copy-done.7, ...), custom_call_target="tpu_custom_call" | custom-call | flops 2200000000 | bytes 10000000 | tf_op jit(solution)/shard_map/stick_project/pallas_call | solution.py:226
  107.6 6.1 %collective-permute-start.37 = (bf16[8,256,128]{2,1,0:T(8,128)(2,1)}, bf16[8,256,128]{2,1,0:T(8,128)(2,1)}, u32[]{:S(2)}, u32[]{:S(2)}) collective-permute-start(bf16[8,256,128]{2,1,0:T(8,128)(2,1)} %get-tuple-element.14.refs_0_), channel_id=1, source_target_pairs={{0,8},{8,16},{16,24},{24,0},{1,9},{9,17},{17,25},{25,1},{2,10},{10... | collective-permute-start | bytes 1572872 | tf_op jit(solution)/shard_map/ppermute | solution.py:446
  118.3 5.8 %collective-permute-done.15.refs_2_ = bf16[128,256]{1,0:T(8,128)(2,1)S(1)} collective-permute-done((bf16[128,256]{1,0:T(8,128)(2,1)S(1)}, bf16[128,256]{1,0:T(8,128)(2,1)S(1)}, u32[]{:S(2)}, u32[]{:S(2)}) %collective-permute-start.15) | collective-permute-done | bytes 65568 | tf_op jit(solution)/shard_map/ppermute | solution.py:478
  124.0 4.0 %collective-permute-start.17 = (bf16[128,256]{1,0:T(8,128)(2,1)S(1)}, bf16[128,256]{1,0:T(8,128)(2,1)S(1)}, u32[]{:S(2)}, u32[]{:S(2)}) collective-permute-start(bf16[128,256]{1,0:T(8,128)(2,1)S(1)} %copy-done.12), channel_id=1, source_target_pairs={{0,96},{32,128},{64,160},{96,192},{128,224},{1,97},{33,129},{65,16... | collective-permute-start | bytes 196616 | tf_op jit(solution)/shard_map/ppermute | solution.py:478
  128.1 6.2 %collective-permute-start.18 = (bf16[128,256]{1,0:T(8,128)(2,1)S(1)}, bf16[128,256]{1,0:T(8,128)(2,1)S(1)}, u32[]{:S(2)}, u32[]{:S(2)}) collective-permute-start(bf16[128,256]{1,0:T(8,128)(2,1)S(1)} %copy-done.12), channel_id=1, source_target_pairs={{0,64},{32,96},{64,128},{96,160},{128,192},{160,224},{1,65},{33,97... | collective-permute-start | bytes 196616 | tf_op jit(solution)/shard_map/ppermute | solution.py:478
  137.5 3.4 %delta_finish.1 = bf16[1024,128]{1,0:T(8,128)(2,1)} custom-call(f32[1,128]{1,0:T(1,128)} %bitcast.55, f32[1024,128]{1,0:T(8,128)} %get-tuple-element.10.qf_ref, f32[1024,128]{1,0:T(8,128)} %get-tuple-element.11.of_ref, bf16[128,256]{1,0:T(8,128)(2,1)} %copy-done.13, bf16[128,256]{1,0:T(8,128)(2,1)} %copy-done.14, bf16[128,256]{1,0:T(8,128)(2,1)} %copy-done.15, ...), custom_call_target="tpu_custom_call" | custom-call | flops 1000000000 | bytes 2000000 | tf_op jit(solution)/shard_map/delta_finish/pallas_call | solution.py:408
  141.0 9.8 %all-to-all-start = ((bf16[8,128,128]{2,1,0:T(8,128)(2,1)}), bf16[8,128,128]{2,1,0:T(8,128)(2,1)S(1)}, u32[]{:S(2)}, u32[]{:S(2)}) async-start(bf16[8,128,128]{2,1,0:T(8,128)(2,1)} %bitcast.48), calls=%async_computation | async-start | bytes 524288 | tf_op jit(solution)/shard_map/all_to_all | solution.py:482
  152.6 3.0 %all-to-all-done = bf16[8,128,128]{2,1,0:T(8,128)(2,1)S(1)} async-done(((bf16[8,128,128]{2,1,0:T(8,128)(2,1)}), bf16[8,128,128]{2,1,0:T(8,128)(2,1)S(1)}, u32[]{:S(2)}, u32[]{:S(2)}) %all-to-all-start) | async-done | bytes 262176 | tf_op jit(solution)/shard_map/all_to_all | solution.py:482
  155.8 33.4 %stick_attention.1 = bf16[16,64,128]{2,1,0:T(8,128)(2,1)} custom-call(s32[384]{0:T(512)} %fusion.17.table, f32[8]{0:T(128)} %off_ref.1, bf16[8,256,128]{2,1,0:T(8,128)(2,1)} %get-tuple-element.13.q, bf16[256,256]{1,0:T(8,128)(2,1)} %constant.55.clone.u_ref, bf16[8,256,128]{2,1,0:T(8,128)(2,1)} %get-tuple-element.14.refs_0_, ...), custom_call_target="tpu_custom_call" | custom-call | flops 20000000000 | bytes 4000000 | tf_op jit(solution)/shard_map/stick_attention/pallas_call | solution.py:147
  189.1 12.1 %all-to-all-start.1 = ((bf16[16,64,128]{2,1,0:T(8,128)(2,1)}), bf16[16,64,128]{2,1,0:T(8,128)(2,1)S(1)}, u32[]{:S(2)}, u32[]{:S(2)}) async-start(bf16[16,64,128]{2,1,0:T(8,128)(2,1)} %stick_attention.1), calls=%async_computation.1 | async-start | bytes 524288 | tf_op jit(solution)/shard_map/all_to_all | solution.py:488
  203.9 9.0 %all-to-all-done.1 = bf16[16,64,128]{2,1,0:T(8,128)(2,1)S(1)} async-done(((bf16[16,64,128]{2,1,0:T(8,128)(2,1)}), bf16[16,64,128]{2,1,0:T(8,128)(2,1)S(1)}, u32[]{:S(2)}, u32[]{:S(2)}) %all-to-all-start.1) | async-done | bytes 262176 | tf_op jit(solution)/shard_map/all_to_all | solution.py:488
  215.8 2.9 %fusion.2 = bf16[1,128,2048]{2,1,0:T(8,128)(2,1)} fusion(f32[128,2048]{1,0:T(8,128)S(1)} %convolution_add_fusion.1, f32[128,2048]{1,0:T(8,128)S(1)} %fusion.4, bf16[512,2048]{1,0:T(8,128)(2,1)} %collective-permute-done.40, bf16[2,128,512]{2,1,0:T(8,128)(2,1)S(1)} %reshape.34, s32[]{:T(128)S(6)} %select_n.26), kind=kOutput, calls=%fused_computation.4 | convolution fusion | flops 269221888 | bytes 4849668 | tf_op jit(solution)/shard_map/dot_general | solution.py:494
  (130 shorter events, 45.8 us)
Async XLA Ops:
  0.0 17.5 %collective-permute-start.21 = (bf16[256,1024]{1,0:T(8,128)(2,1)}, bf16[256,1024]{1,0:T(8,128)(2,1)}, u32[]{:S(2)}, u32[]{:S(2)}) collective-permute-start(bf16[256,1024]{1,0:T(8,128)(2,1)} %bitcast.40), channel_id=1, source_target_pairs={{0,32},{32,64},{64,96},{96,128},{128,160},{160,192},{192,224},{224... | collective-permute-start | bytes 1572872 | tf_op jit(solution)/shard_map/ppermute | solution.py:455
  1.6 18.9 %collective-permute-start.22 = (bf16[256,1024]{1,0:T(8,128)(2,1)}, bf16[256,1024]{1,0:T(8,128)(2,1)S(1)}, u32[]{:S(2)}, u32[]{:S(2)}) collective-permute-start(bf16[256,1024]{1,0:T(8,128)(2,1)} %bitcast.41), channel_id=1, source_target_pairs={{0,224},{32,0},{64,32},{96,64},{128,96},{160,128},{192,160},{224,1... | collective-permute-start | bytes 1572872 | tf_op jit(solution)/shard_map/ppermute | solution.py:455
  17.5 24.7 %collective-permute-start.8 = (bf16[256,1024]{1,0:T(8,128)(2,1)}, bf16[256,1024]{1,0:T(8,128)(2,1)}, u32[]{:S(2)}, u32[]{:S(2)}) collective-permute-start(bf16[256,1024]{1,0:T(8,128)(2,1)} %bitcast.45), channel_id=1, source_target_pairs={{0,24},{8,0},{16,8},{24,16},{1,25},{9,1},{17,9},{25,17},{2,26},{10... | collective-permute-start | bytes 1572872 | tf_op jit(solution)/shard_map/ppermute | solution.py:446
  20.6 24.1 %collective-permute-start.3 = (bf16[512,640]{1,0:T(8,128)(2,1)S(1)}, bf16[512,640]{1,0:T(8,128)(2,1)S(1)}, u32[]{:S(2)}, u32[]{:S(2)}) collective-permute-start(bf16[512,640]{1,0:T(8,128)(2,1)S(1)} %concatenate.3.refs_4_.refs_0_), channel_id=1, source_target_pairs={{0,2},{2,4},{4,6},{6,0},{1,3},{3,5},{5,7},{7,1},{8,10},{10,12},{12... | collective-permute-start | bytes 1966088 | tf_op jit(solution)/shard_map/ppermute | solution.py:446
  21.9 23.6 %collective-permute-start.23 = (bf16[256,1024]{1,0:T(8,128)(2,1)}, bf16[256,1024]{1,0:T(8,128)(2,1)}, u32[]{:S(2)}, u32[]{:S(2)}) collective-permute-start(bf16[256,1024]{1,0:T(8,128)(2,1)} %collective-permute-done.21.refs_5_), channel_id=1, source_target_pairs={{0,32},{32,64},{64,96},{96,128},{128,160},{160,192},{192,224},{224... | collective-permute-start | bytes 1572872 | tf_op jit(solution)/shard_map/ppermute | solution.py:458
  22.5 23.0 %collective-permute-start.24 = (bf16[256,1024]{1,0:T(8,128)(2,1)S(1)}, bf16[256,1024]{1,0:T(8,128)(2,1)S(1)}, u32[]{:S(2)}, u32[]{:S(2)}) collective-permute-start(bf16[256,1024]{1,0:T(8,128)(2,1)S(1)} %collective-permute-done.22.refs_6_), channel_id=1, source_target_pairs={{0,224},{32,0},{64,32},{96,64},{128,96},{160,128},{192,160},{224,1... | collective-permute-start | bytes 1572872 | tf_op jit(solution)/shard_map/ppermute | solution.py:458
  28.8 22.8 %collective-permute-start.4 = (bf16[512,640]{1,0:T(8,128)(2,1)S(1)}, bf16[512,640]{1,0:T(8,128)(2,1)S(1)}, u32[]{:S(2)}, u32[]{:S(2)}) collective-permute-start(bf16[512,640]{1,0:T(8,128)(2,1)S(1)} %concatenate.3.refs_4_.refs_0_), channel_id=1, source_target_pairs={{0,4},{2,6},{4,0},{6,2},{1,5},{3,7},{5,1},{7,3},{8,12},{10,14},{12... | collective-permute-start | bytes 1966088 | tf_op jit(solution)/shard_map/ppermute | solution.py:446
  42.2 19.5 %collective-permute-start.5 = (bf16[512,640]{1,0:T(8,128)(2,1)S(1)}, bf16[512,640]{1,0:T(8,128)(2,1)S(1)}, u32[]{:S(2)}, u32[]{:S(2)}) collective-permute-start(bf16[512,640]{1,0:T(8,128)(2,1)S(1)} %concatenate.3.refs_4_.refs_0_), channel_id=1, source_target_pairs={{0,6},{2,0},{4,2},{6,4},{1,7},{3,1},{5,3},{7,5},{8,14},{10,8},{12,... | collective-permute-start | bytes 1966088 | tf_op jit(solution)/shard_map/ppermute | solution.py:446
  44.7 18.2 %collective-permute-start.29 = (bf16[256,1024]{1,0:T(8,128)(2,1)}, bf16[256,1024]{1,0:T(8,128)(2,1)S(1)}, u32[]{:S(2)}, u32[]{:S(2)}) collective-permute-start(bf16[256,1024]{1,0:T(8,128)(2,1)} %collective-permute-done.21.refs_5_), channel_id=1, source_target_pairs={{0,1},{1,0},{2,3},{3,2},{4,5},{5,4},{6,7},{7,6},{8,9},{9,8},{10,11... | collective-permute-start | bytes 1572872 | tf_op jit(solution)/shard_map/ppermute | solution.py:444
  45.5 17.6 %collective-permute-start.25 = (bf16[256,1024]{1,0:T(8,128)(2,1)}, bf16[256,1024]{1,0:T(8,128)(2,1)S(1)}, u32[]{:S(2)}, u32[]{:S(2)}) collective-permute-start(bf16[256,1024]{1,0:T(8,128)(2,1)} %collective-permute-done.23.refs_7_), channel_id=1, source_target_pairs={{0,32},{32,64},{64,96},{96,128},{128,160},{160,192},{192,224},{224... | collective-permute-start | bytes 1572872 | tf_op jit(solution)/shard_map/ppermute | solution.py:459
  45.5 17.9 %collective-permute-start.26 = (bf16[256,1024]{1,0:T(8,128)(2,1)S(1)}, bf16[256,1024]{1,0:T(8,128)(2,1)S(1)}, u32[]{:S(2)}, u32[]{:S(2)}) collective-permute-start(bf16[256,1024]{1,0:T(8,128)(2,1)S(1)} %collective-permute-done.24.refs_8_), channel_id=1, source_target_pairs={{0,224},{32,0},{64,32},{96,64},{128,96},{160,128},{192,160},{224,1... | collective-permute-start | bytes 1572872 | tf_op jit(solution)/shard_map/ppermute | solution.py:459
  68.8 24.9 %collective-permute-start.32 = (bf16[256,1024]{1,0:T(8,128)(2,1)}, bf16[256,1024]{1,0:T(8,128)(2,1)}, u32[]{:S(2)}, u32[]{:S(2)}) collective-permute-start(bf16[256,1024]{1,0:T(8,128)(2,1)} %copy-done.10), channel_id=1, source_target_pairs={{0,1},{1,0},{2,3},{3,2},{4,5},{5,4},{6,7},{7,6},{8,9},{9,8},{10,11... | collective-permute-start | bytes 1572872 | tf_op jit(solution)/shard_map/ppermute | solution.py:444
  69.7 28.7 %collective-permute-start.33 = (bf16[256,1024]{1,0:T(8,128)(2,1)S(1)}, bf16[256,1024]{1,0:T(8,128)(2,1)}, u32[]{:S(2)}, u32[]{:S(2)}) collective-permute-start(bf16[256,1024]{1,0:T(8,128)(2,1)S(1)} %collective-permute-done.25.refs_9_), channel_id=1, source_target_pairs={{0,1},{1,0},{2,3},{3,2},{4,5},{5,4},{6,7},{7,6},{8,9},{9,8},{10,11... | collective-permute-start | bytes 1572872 | tf_op jit(solution)/shard_map/ppermute | solution.py:444
  69.8 28.7 %collective-permute-start.34 = (bf16[256,1024]{1,0:T(8,128)(2,1)S(1)}, bf16[256,1024]{1,0:T(8,128)(2,1)}, u32[]{:S(2)}, u32[]{:S(2)}) collective-permute-start(bf16[256,1024]{1,0:T(8,128)(2,1)S(1)} %collective-permute-done.26.refs_10_), channel_id=1, source_target_pairs={{0,1},{1,0},{2,3},{3,2},{4,5},{5,4},{6,7},{7,6},{8,9},{9,8},{10,11... | collective-permute-start | bytes 1572872 | tf_op jit(solution)/shard_map/ppermute | solution.py:444
  74.6 23.8 %collective-permute-start.35 = (bf16[128,1024]{1,0:T(8,128)(2,1)}, bf16[128,1024]{1,0:T(8,128)(2,1)}, u32[]{:S(2)}, u32[]{:S(2)}) collective-permute-start(bf16[128,1024]{1,0:T(8,128)(2,1)} %collective-permute-done.27.refs_11_), channel_id=1, source_target_pairs={{0,1},{1,0},{2,3},{3,2},{4,5},{5,4},{6,7},{7,6},{8,9},{9,8},{10,11... | collective-permute-start | bytes 786440 | tf_op jit(solution)/shard_map/ppermute | solution.py:444
  75.8 22.6 %collective-permute-start.36 = (bf16[128,1024]{1,0:T(8,128)(2,1)}, bf16[128,1024]{1,0:T(8,128)(2,1)}, u32[]{:S(2)}, u32[]{:S(2)}) collective-permute-start(bf16[128,1024]{1,0:T(8,128)(2,1)} %collective-permute-done.28.refs_12_), channel_id=1, source_target_pairs={{0,1},{1,0},{2,3},{3,2},{4,5},{5,4},{6,7},{7,6},{8,9},{9,8},{10,11... | collective-permute-start | bytes 786440 | tf_op jit(solution)/shard_map/ppermute | solution.py:444
  93.7 21.9 %collective-permute-start.13 = (bf16[128,256]{1,0:T(8,128)(2,1)}, bf16[128,256]{1,0:T(8,128)(2,1)S(1)}, u32[]{:S(2)}, u32[]{:S(2)}) collective-permute-start(bf16[128,256]{1,0:T(8,128)(2,1)} %get-tuple-element.12), channel_id=1, source_target_pairs={{0,224},{1,225},{2,226},{3,227},{4,228},{5,229},{6,230},{7,231},{8... | collective-permute-start | bytes 196616 | tf_op jit(solution)/shard_map/ppermute | solution.py:478
  107.6 48.2 %collective-permute-start.37 = (bf16[8,256,128]{2,1,0:T(8,128)(2,1)}, bf16[8,256,128]{2,1,0:T(8,128)(2,1)}, u32[]{:S(2)}, u32[]{:S(2)}) collective-permute-start(bf16[8,256,128]{2,1,0:T(8,128)(2,1)} %get-tuple-element.14.refs_0_), channel_id=1, source_target_pairs={{0,8},{8,16},{16,24},{24,0},{1,9},{9,17},{17,25},{25,1},{2,10},{10... | collective-permute-start | bytes 1572872 | tf_op jit(solution)/shard_map/ppermute | solution.py:446
  113.6 42.1 %collective-permute-start.38 = (bf16[8,256,128]{2,1,0:T(8,128)(2,1)}, bf16[8,256,128]{2,1,0:T(8,128)(2,1)}, u32[]{:S(2)}, u32[]{:S(2)}) collective-permute-start(bf16[8,256,128]{2,1,0:T(8,128)(2,1)} %get-tuple-element.14.refs_0_), channel_id=1, source_target_pairs={{0,16},{8,24},{16,0},{24,8},{1,17},{9,25},{17,1},{25,9},{2,18},{10... | collective-permute-start | bytes 1572872 | tf_op jit(solution)/shard_map/ppermute | solution.py:446
  114.2 41.6 %collective-permute-start.39 = (bf16[8,256,128]{2,1,0:T(8,128)(2,1)}, bf16[8,256,128]{2,1,0:T(8,128)(2,1)}, u32[]{:S(2)}, u32[]{:S(2)}) collective-permute-start(bf16[8,256,128]{2,1,0:T(8,128)(2,1)} %get-tuple-element.14.refs_0_), channel_id=1, source_target_pairs={{0,24},{8,0},{16,8},{24,16},{1,25},{9,1},{17,9},{25,17},{2,26},{10... | collective-permute-start | bytes 1572872 | tf_op jit(solution)/shard_map/ppermute | solution.py:446
  141.0 14.6 %all-to-all-start = ((bf16[8,128,128]{2,1,0:T(8,128)(2,1)}), bf16[8,128,128]{2,1,0:T(8,128)(2,1)S(1)}, u32[]{:S(2)}, u32[]{:S(2)}) async-start(bf16[8,128,128]{2,1,0:T(8,128)(2,1)} %bitcast.48), calls=%async_computation | async-start | bytes 524288 | tf_op jit(solution)/shard_map/all_to_all | solution.py:482
  150.8 51.0 %collective-permute-start.20 = (bf16[512,2048]{1,0:T(8,128)(2,1)S(1)}, bf16[512,2048]{1,0:T(8,128)(2,1)}, u32[]{:S(2)}, u32[]{:S(2)}) collective-permute-start(bf16[512,2048]{1,0:T(8,128)(2,1)S(1)} %copy-done.2), channel_id=1, source_target_pairs={{0,1},{1,0},{2,3},{3,2},{4,5},{5,4},{6,7},{7,6},{8,9},{9,8},{10,11... | collective-permute-start | bytes 6291464 | tf_op jit(solution)/shard_map/ppermute | solution.py:444
  151.2 64.7 %collective-permute-start.40 = (bf16[512,2048]{1,0:T(8,128)(2,1)}, bf16[512,2048]{1,0:T(8,128)(2,1)}, u32[]{:S(2)}, u32[]{:S(2)}) collective-permute-start(bf16[512,2048]{1,0:T(8,128)(2,1)} %param.32), channel_id=1, source_target_pairs={{0,1},{1,0},{2,3},{3,2},{4,5},{5,4},{6,7},{7,6},{8,9},{9,8},{10,11... | collective-permute-start | bytes 6291464 | tf_op jit(solution)/shard_map/ppermute | solution.py:444
  189.1 23.7 %all-to-all-start.1 = ((bf16[16,64,128]{2,1,0:T(8,128)(2,1)}), bf16[16,64,128]{2,1,0:T(8,128)(2,1)S(1)}, u32[]{:S(2)}, u32[]{:S(2)}) async-start(bf16[16,64,128]{2,1,0:T(8,128)(2,1)} %stick_attention.1), calls=%async_computation.1 | async-start | bytes 524288 | tf_op jit(solution)/shard_map/all_to_all | solution.py:488
  (42 other events, 661.5 us)
